TPU v7x, 256 devices: a whole 4x4x8 slice. The times are simulated.
256 devices in a mesh: ep: 128 (over z, y, x), tp: 2 (over core).
Axes of the slice: x: 4, y: 4, z: 8, core: 2. Of those that a mesh axis runs over, the one named last changes fastest.
Arguments:
- tokens: bfloat16 [2048, 2048], P('ep', 'tp'), may hold values from -6 to 6
- state: float32 [2048, 4, 128, 128], P('ep', 'tp'), may hold values from -4 to 4
- norm_mix: float32 [2048], replicated, may hold values from 0.1 to 1.9
- w_query: bfloat16 [2048, 512], P(None, 'tp'), may hold values from -0.125 to 0.125
- w_key: bfloat16 [2048, 512], P(None, 'tp'), may hold values from -0.125 to 0.125
- w_value: bfloat16 [2048, 512], P(None, 'tp'), may hold values from -0.125 to 0.125
- w_out: bfloat16 [512, 2048], P('tp'), may hold values from -0.25 to 0.25
- norm_ffn: float32 [2048], P('tp'), may hold values from 0.1 to 1.9
- gate_vector: bfloat16 [2048], P('tp'), may hold values from -0.125 to 0.125
- dense_gate: bfloat16 [2048, 2816], P('tp', 'ep'), may hold values from -0.125 to 0.125
- dense_up: bfloat16 [2048, 2816], P('tp', 'ep'), may hold values from -0.125 to 0.125
- dense_down: bfloat16 [2816, 2048], P('ep', 'tp'), may hold values from -0.109375 to 0.109375
- exp_gate: bfloat16 [128, 2048, 176], P('ep', None, 'tp'), may hold values from -0.125 to 0.125
- exp_up: bfloat16 [128, 2048, 176], P('ep', None, 'tp'), may hold values from -0.125 to 0.125
- exp_down: bfloat16 [128, 176, 2048], P('ep', 'tp'), may hold values from -0.109375 to 0.109375
- routes: int32 [2048, 2], P('ep'), may hold values from 0 to 7, all different within a row; in each aligned block of 16 rows (0 to 15, 16 to 31, ...) at most 5 rows name the same one
- route_w: bfloat16 [2048, 2], P('ep'), may hold values from 0.099609375 to 1
Outputs:
- mixed: bfloat16 [2048, 2048], P('ep', 'tp')
- new_state: float32 [2048, 4, 128, 128], P('ep', 'tp')
Inputs may be any that keep to these rules, and one draw needn't show every extreme that they name: `routes`: each row names 2 different experts. Within the rows of one device (aligned blocks of 16 rows) no expert is named by more than 5 rows, a bound that some blocks reach.
All inputs are finite; a program needn't handle non-finite values.
Results may differ from a plain program's by a relative error of at most 0.014.
Values may be sent and summed in bfloat16 or wider, within the bound.
A program may use at most 128 MiB of HBM per device.

v0:
```python
import jax
import jax.numpy as jnp
from jax import lax
from jax.sharding import Mesh
from jax.sharding import PartitionSpec as P

EXPERTS = 8
TOPK = 2
CAP = 5
EP = ("ep_0", "ep_1", "ep_2")


epsilon = 1e-06


def copy_for_each(value, axis):
    copies = jnp.broadcast_to(value, (lax.axis_size(axis), *value.shape))
    return lax.all_to_all(copies, axis, split_axis=0, concat_axis=0, tiled=True)


def in_order(tiles, dim):
    tiles = jnp.moveaxis(tiles, 0, dim)
    shape = tiles.shape
    return tiles.reshape(*shape[:dim], shape[dim] * shape[dim + 1], *shape[dim + 2 :])


def gather_directly(value, axis, dim):
    tiles = copy_for_each(value, axis)
    return in_order(tiles, dim)


def cut_along(value, dim, size):
    shape = value.shape
    tiles = value.reshape(*shape[:dim], size, shape[dim] // size, *shape[dim + 1 :])
    return jnp.moveaxis(tiles, dim, 0)


def sum_at_owner(value, axis, dim):
    size = lax.axis_size(axis)
    tiles = lax.all_to_all(cut_along(value, dim, size), axis, 0, 0, tiled=True)
    return jnp.sum(tiles.astype(jnp.float32), axis=0)


def taken_together(value, axis):
    everything = copy_for_each(value, axis)
    return jnp.sum(everything.astype(jnp.float32), axis=0)


def side_by_side(arrays, axis, dim, along):
    widths = [a.shape[along] for a in arrays]
    both = jnp.concatenate(arrays, axis=along)
    filled = lax.all_gather(both, axis, axis=dim, tiled=True)
    return tuple(jnp.split(filled, [sum(widths[:k]) for k in range(1, len(widths))], axis=along))


def whole_of(value, axes, dim):
    for axis in reversed(axes):
        value = lax.all_gather(value, axis, axis=dim, tiled=True)
    return value


def summed_rows(total, axes):
    for axis in axes:
        total = lax.psum_scatter(total, axis, scatter_dimension=0, tiled=True)
    return total


def route_tables(routes, route_w):
    onehot = (routes[:, :, None] == jnp.arange(EXPERTS, dtype=jnp.int32)[None, None, :]).astype(
        jnp.float32
    )
    member = jnp.sum(onehot, axis=1)
    weight = jnp.sum(onehot * route_w.astype(jnp.float32)[:, :, None], axis=1)
    place = jnp.cumsum(member, axis=0) - member
    slot_ids = jnp.arange(CAP, dtype=jnp.float32)
    select = member.T[:, None, :] * (place.T[:, None, :] == slot_ids[None, :, None]).astype(
        jnp.float32
    )
    return (select, weight)


def expert_math(flat_rows, weights):
    gate_pre = jnp.dot(flat_rows, weights[0], preferred_element_type=jnp.float32)
    up_part = jnp.dot(flat_rows, weights[1], preferred_element_type=jnp.float32)
    hidden = (jax.nn.silu(gate_pre) * up_part).astype(jnp.bfloat16)
    return jnp.dot(hidden, weights[2], preferred_element_type=jnp.float32)


def expert_apply(slot_rows, weights):
    full_rows = gather_directly(slot_rows, "tp", 2)
    row_count = full_rows.shape[0] * full_rows.shape[1]
    partial_value = expert_math(full_rows.reshape(row_count, full_rows.shape[2]), weights)
    summed = sum_at_owner(partial_value.astype(jnp.bfloat16), "tp", 1)
    return summed.reshape(slot_rows.shape[0], slot_rows.shape[1], summed.shape[1])


def body(
    tokens,
    state,
    norm_mix,
    w_query,
    w_key,
    w_value,
    w_out,
    norm_ffn,
    gate_vector,
    dense_gate,
    dense_up,
    dense_down,
    exp_gate,
    exp_up,
    exp_down,
    routes,
    route_w,
):
    row_count, half_width = tokens.shape
    heads_here, head_size = (state.shape[1], state.shape[2])
    weights = (exp_gate[0], exp_up[0], exp_down[0])
    full_x = gather_directly(tokens, "tp", 1)
    width = full_x.shape[1]
    full_f = full_x.astype(jnp.float32)
    normed = (
        full_f
        * lax.rsqrt(jnp.sum(full_f * full_f, axis=1, keepdims=True) / width + epsilon)
        * norm_mix
    ).astype(jnp.bfloat16)
    query = jnp.dot(normed, w_query, preferred_element_type=jnp.float32).astype(jnp.bfloat16)
    key_rows = jnp.dot(normed, w_key, preferred_element_type=jnp.float32).astype(jnp.bfloat16)
    value_rows = jnp.dot(normed, w_value, preferred_element_type=jnp.float32).astype(jnp.bfloat16)
    query3 = query.astype(jnp.float32).reshape(row_count, heads_here, head_size)
    key3 = key_rows.astype(jnp.float32).reshape(row_count, heads_here, head_size) * head_size ** (
        -0.5
    )
    value3 = value_rows.astype(jnp.float32).reshape(row_count, heads_here, head_size)
    head_ids = (lax.axis_index("tp") * heads_here + jnp.arange(heads_here, dtype=jnp.int32)).astype(
        jnp.float32
    )
    decay = 1.0 - jnp.exp2(-3.0 - 2.0 * head_ids)
    new_state = decay[None, :, None, None] * state + jnp.einsum("shd,she->shde", key3, value3)
    read = jnp.einsum("shd,shde->she", query3, new_state)
    centre = jnp.mean(read, axis=2, keepdims=True)
    spread = jnp.mean(jnp.square(read - centre), axis=2, keepdims=True)
    heads_out = (
        ((read - centre) * lax.rsqrt(spread + epsilon))
        .astype(jnp.bfloat16)
        .reshape(row_count, heads_here * head_size)
    )
    mix_part = jnp.dot(heads_out, w_out, preferred_element_type=jnp.float32)
    mix_sum = taken_together(mix_part.astype(jnp.bfloat16), "tp").astype(jnp.float32)
    after_full = (full_f + mix_sum).astype(jnp.bfloat16)
    after_ff = after_full.astype(jnp.float32)
    squares = jnp.sum(after_ff * after_ff, axis=1, keepdims=True)
    after = lax.dynamic_slice_in_dim(after_full, lax.axis_index("tp") * half_width, half_width, 1)
    after_f = after.astype(jnp.float32)
    normed2 = (after_f * lax.rsqrt(squares / width + epsilon) * norm_ffn).astype(jnp.bfloat16)
    all_rows, all_weights = side_by_side((normed2, route_w), EP, 0, 1)
    all_routes = whole_of(routes, EP, 0)
    dense_pre = jnp.dot(all_rows, dense_gate, preferred_element_type=jnp.float32)
    up_pre = jnp.dot(all_rows, dense_up, preferred_element_type=jnp.float32)
    logit = jnp.dot(all_rows, gate_vector, preferred_element_type=jnp.float32)
    dense_pre, up_pre, logit = (
        taken_together(dense_pre.astype(jnp.bfloat16), "tp").astype(jnp.float32),
        taken_together(up_pre.astype(jnp.bfloat16), "tp").astype(jnp.float32),
        taken_together(logit.astype(jnp.bfloat16), "tp").astype(jnp.float32),
    )
    dense_hidden = (jax.nn.sigmoid(logit)[:, None] * jax.nn.silu(dense_pre) * up_pre).astype(
        jnp.bfloat16
    )
    ep_count = lax.axis_size(EP)
    group_size = ep_count // EXPERTS
    block_select, block_weight = jax.vmap(route_tables)(
        all_routes.reshape(ep_count, row_count, TOPK),
        all_weights.reshape(ep_count, row_count, TOPK),
    )
    own_expert = lax.axis_index(EP) // group_size
    select_mine = lax.dynamic_index_in_dim(block_select, own_expert, axis=1, keepdims=False)
    weight_mine = lax.dynamic_index_in_dim(block_weight, own_expert, axis=2, keepdims=False)
    slot_rows = jnp.einsum(
        "ncr,nrd->ncd",
        select_mine.astype(jnp.bfloat16),
        all_rows.reshape(ep_count, row_count, half_width),
        preferred_element_type=jnp.float32,
    ).astype(jnp.bfloat16)
    expert_out = expert_apply(slot_rows, weights)
    extra_term = jnp.einsum(
        "ncr,ncd->nrd", select_mine * weight_mine[:, None, :], expert_out
    ).reshape(ep_count * row_count, half_width)
    value = jnp.dot(dense_hidden, dense_down, preferred_element_type=jnp.float32)
    value = value + extra_term
    combined = summed_rows(value, EP)
    return ((after_f + combined).astype(jnp.bfloat16), new_state)


def solution(mesh):
    finer = Mesh(mesh.devices.reshape(8, 4, 4, mesh.shape["tp"]), ("ep_0", "ep_1", "ep_2", "tp"))
    in_specs = (
        P(EP, "tp"),
        P(EP, "tp", None, None),
        P(),
        P(None, "tp"),
        P(None, "tp"),
        P(None, "tp"),
        P("tp", None),
        P("tp"),
        P("tp"),
        P("tp", EP),
        P("tp", EP),
        P(EP, "tp"),
        P(EP, None, "tp"),
        P(EP, None, "tp"),
        P(EP, "tp", None),
        P(EP, None),
        P(EP, None),
    )
    out_specs = (P(EP, "tp"), P(EP, "tp", None, None))
    return jax.shard_map(body, mesh=finer, in_specs=in_specs, out_specs=out_specs, check_vma=False)
```

profile of v0, /device:TPU:1, one launch (start us, length us, event | category | flops | bytes accessed | tf_op | source)
XLA Modules:
  0.0 375.0 jit_solution(9884479791127990557)
XLA Ops:
  8.7 6.5 %all-to-all-start = ((bf16[2,16,1024]{2,1,0:T(8,128)(2,1)}), bf16[2,16,1024]{2,1,0:T(8,128)(2,1)S(1)}, u32[]{:S(2)}, u32[]{:S(2)}) async-start(bf16[2,16,1024]{2,1,0:T(8,128)(2,1)} %broadcast_in_dim.12), calls=%async_computation | async-start | bytes 131072 | tf_op jit(solution)/shard_map/all_to_all | solution.py:18
  25.5 3.7 all-to-all-start.1
  31.3 6.0 %all-gather = s32[4,16,2]{1,2,0:T(2,128)S(1)} all-gather(s32[1,16,2]{1,2,0:T(2,128)S(1)} %bitcast.110), channel_id=1, replica_groups=mesh['ep_0'=8,'ep_1'=4,'ep_2'=4,'tp'=2] {'ep_2'}, dimensions={0}, use_global_device_ids=true | all-gather | bytes 640 | tf_op jit(solution)/shard_map/all_gather | solution.py:58
  37.4 8.0 %all-gather.1 = s32[4,64,2]{1,2,0:T(2,128)S(1)} all-gather(s32[1,64,2]{1,2,0:T(2,128)S(1)} %reshape.110), channel_id=1, replica_groups=mesh['ep_0'=8,'ep_1'=4,'ep_2'=4,'tp'=2] {'ep_1'}, dimensions={0}, use_global_device_ids=true | all-gather | bytes 2560 | tf_op jit(solution)/shard_map/all_gather | solution.py:58
  45.4 20.8 %all_gather.15 = s32[2048,2]{0,1:T(2,128)S(1)} all-gather(s32[256,2]{0,1:T(2,128)S(1)} %reshape.111), channel_id=1, replica_groups=mesh['ep_0'=8,'ep_1'=4,'ep_2'=4,'tp'=2] {'ep_0'}, dimensions={0}, use_global_device_ids=true | all-gather | bytes 18432 | tf_op jit(solution)/shard_map/all_gather | solution.py:58
  66.4 81.4 %all-gather.4.cloned.1.call-done = bf16[2048,1026]{1,0:T(8,128)(2,1)} async-done(((bf16[16,1026]{1,0:T(8,128)(2,1)}), bf16[2048,1026]{1,0:T(8,128)(2,1)}) %all-gather.4.cloned.1.call-update) | async-done | bytes 4202512 | tf_op jit(solution)/shard_map/all_gather | solution.py:52
  147.8 3.4 fusion.42
  152.5 8.0 %all_to_all.36 = bf16[2,2,1024]{2,1,0:T(2,128)(2,1)S(1)} all-to-all(bf16[2,2,1024]{2,1,0:T(2,128)(2,1)S(1)} %reshape.119), channel_id=1, replica_groups=mesh['ep_0'=8,'ep_1'=4,'ep_2'=4,'tp'=2] {'tp'}, dimensions={0} | all-to-all | bytes 16384 | tf_op jit(solution)/shard_map/all_to_all | solution.py:18
  162.4 2.2 slice-done.3
  166.5 5.9 %all_to_all.37 = bf16[2,128,5,1024]{3,1,2,0:T(8,128)(2,1)S(1)} all-to-all(bf16[2,128,5,1024]{3,1,2,0:T(8,128)(2,1)S(1)} %broadcast_in_dim.17), channel_id=1, replica_groups=mesh['ep_0'=8,'ep_1'=4,'ep_2'=4,'tp'=2] {'tp'}, dimensions={0} | all-to-all | bytes 5242880 | tf_op jit(solution)/shard_map/all_to_all | solution.py:18
  172.3 2.7 copy.123
  178.3 5.2 %convolution_convert_fusion = bf16[640,2048]{1,0:T(8,128)(2,1)} fusion(bf16[640,2048]{1,0:T(8,128)(2,1)} %bitcast.91, bf16[1,88,2048]{2,1,0:T(8,128)(2,1)S(1)} %copy-done.5, bf16[1,2048,88]{1,2,0:T(8,128)(2,1)S(1)} %copy-done.6, f32[640,88]{0,1:T(8,128)S(1)} %fusion.9), kind=kOutput, calls=%fused_computation.2 | convolution fusion | flops 463022080 | bytes 6189056 | tf_op jit(solution)/shard_map/dot_general | solution.py:86
  183.5 3.6 copy.145
  187.1 5.4 %all-to-all-start.6 = ((bf16[2,640,1024]{2,1,0:T(8,128)(2,1)}), bf16[2,640,1024]{2,1,0:T(8,128)(2,1)}, u32[]{:S(2)}, u32[]{:S(2)}) async-start(bf16[2,640,1024]{2,1,0:T(8,128)(2,1)} %bitcast.96), calls=%async_computation.6 | async-start | bytes 5242880 | tf_op jit(solution)/shard_map/all_to_all | solution.py:40
  192.5 3.4 convolution_convert_fusion.2
  196.6 3.4 all-to-all-start.3
  200.1 2.3 convert_reduce_fusion
  202.4 1.6 reshape.103
  204.0 6.3 %fusion.5 = f32[128,16,1024]{2,1,0:T(8,128)} fusion(bf16[128,5,1024]{2,1,0:T(8,128)(2,1)} %reshape.103, f32[128,1,16]{2,0,1:T(8,128)S(1)} %get-tuple-element.7, f32[128,1,16]{2,0,1:T(8,128)S(1)} %get-tuple-element.6, f32[128,16]{1,0:T(8,128)S(1)} %copy.121), kind=kOutput, calls=%fused_computation.22 | convolution fusion | flops 21002240 | bytes 9723904 | tf_op jit(solution)/shard_map/ncr,ncd->nrd/dot_general | solution.py:185
  212.2 3.4 all-to-all-start.4
  216.8 7.9 %bitcast_add_fusion = f32[2048,1024]{1,0:T(8,128)} fusion(f32[128,16,1024]{2,1,0:T(8,128)} %fusion.5, bf16[22,1024]{1,0:T(8,128)(2,1)S(1)} %copy-done.7, f32[2048,22]{0,1:T(8,128)S(1)} %convert_reduce_fusion.1, f32[2048,22]{0,1:T(8,128)S(1)} %convert_reduce_fusion.2, f32[2048]{0:T(1024)S(1)} %add_divide_fusion), kind=kOutput, calls=%fused_computation | convolution fusion | flops 94687232 | bytes 17190912 | tf_op jit(solution)/shard_map/dot_general | solution.py:188
  224.8 91.5 %reduce-scatter.4.cloned.1.call-done = f32[256,1024]{1,0:T(8,128)} async-done(((f32[2048,1024]{1,0:T(8,128)}), f32[256,1024]{1,0:T(8,128)}) %reduce-scatter.4.cloned.1.call-update) | async-done | bytes 1048592 | tf_op jit(solution)/shard_map/reduce_scatter | solution.py:64
  316.3 26.1 %reduce-scatter.6.cloned.1.call-done = f32[64,1024]{1,0:T(8,128)} async-done(((f32[256,1024]{1,0:T(8,128)}), f32[64,1024]{1,0:T(8,128)}) %reduce-scatter.6.cloned.1.call-update) | async-done | bytes 262160 | tf_op jit(solution)/shard_map/reduce_scatter | solution.py:64
  342.4 24.6 %reduce-scatter.8.cloned.1.call-done = f32[16,1024]{1,0:T(8,128)} async-done(((f32[64,1024]{1,0:T(8,128)}), f32[16,1024]{1,0:T(8,128)}) %reduce-scatter.8.cloned.1.call-update) | async-done | bytes 65552 | tf_op jit(solution)/shard_map/reduce_scatter | solution.py:64
  (111 shorter events, 27.6 us)
Async XLA Ops:
  7.2 17.4 %copy-start = (bf16[256,2048]{1,0:T(8,128)(2,1)S(1)}, bf16[256,2048]{1,0:T(8,128)(2,1)}, u32[]{:S(2)}) copy-start(bf16[256,2048]{1,0:T(8,128)(2,1)} %param.23) | copy-start | bytes 3145732
  7.2 14.6 %copy-start.3 = (f32[16,2,128,128]{3,2,1,0:T(8,128)S(1)}, f32[16,2,128,128]{3,2,1,0:T(8,128)}, u32[]{:S(2)}) copy-start(f32[16,2,128,128]{3,2,1,0:T(8,128)} %param.18) | copy-start | bytes 6291460
  8.7 7.6 %all-to-all-start = ((bf16[2,16,1024]{2,1,0:T(8,128)(2,1)}), bf16[2,16,1024]{2,1,0:T(8,128)(2,1)S(1)}, u32[]{:S(2)}, u32[]{:S(2)}) async-start(bf16[2,16,1024]{2,1,0:T(8,128)(2,1)} %broadcast_in_dim.12), calls=%async_computation | async-start | bytes 131072 | tf_op jit(solution)/shard_map/all_to_all | solution.py:18
  23.8 5.4 %copy-start.11 = (bf16[16,2]{0,1:T(2,128)(2,1)S(1)}, bf16[16,2]{0,1:T(2,128)(2,1)}, u32[]{:S(2)}) copy-start(bf16[16,2]{0,1:T(2,128)(2,1)} %param.33) | copy-start | bytes 196
  23.8 6.7 %copy-start.8 = (f32[1024]{0:T(1024)S(1)}, f32[1024]{0:T(1024)}, u32[]{:S(2)}) copy-start(f32[1024]{0:T(1024)} %param.24) | copy-start | bytes 12292
  23.8 7.4 %copy-start.9 = (bf16[1024]{0:T(1024)(128)(2,1)S(1)}, bf16[1024]{0:T(1024)(128)(2,1)}, u32[]{:S(2)}) copy-start(bf16[1024]{0:T(1024)(128)(2,1)} %param.25) | copy-start | bytes 6148
  23.8 7.5 %copy-start.10 = (s32[16,2]{0,1:T(2,128)S(1)}, s32[16,2]{0,1:T(2,128)}, u32[]{:S(2)}) copy-start(s32[16,2]{0,1:T(2,128)} %param.32) | copy-start | bytes 388
  25.5 4.8 %all-to-all-start.1 = ((bf16[2,16,2048]{2,1,0:T(8,128)(2,1)}), bf16[2,16,2048]{2,1,0:T(8,128)(2,1)S(1)}, u32[]{:S(2)}, u32[]{:S(2)}) async-start(bf16[2,16,2048]{2,1,0:T(8,128)(2,1)} %broadcast_in_dim.13), calls=%async_computation.1 | async-start | bytes 262144 | tf_op jit(solution)/shard_map/all_to_all | solution.py:18
  29.2 118.6 %all-gather.4.cloned.1.call-start = ((), (), s32[]{:S(2)}) async-start(), calls=%async_computation.10 | async-start | bytes 4755456 | tf_op jit(solution)/shard_map/all_gather | solution.py:52
  147.8 12.8 %slice-start.2 = ((bf16[2048,1026]{1,0:T(8,128)(2,1)}), bf16[2048,2]{1,0:T(8,128)(2,1)S(1)}, s32[]{:S(2)}) async-start(bf16[2048,1026]{1,0:T(8,128)(2,1)} %all-gather.4.cloned.1.call-done), calls=%async_computation.16 | async-start | bytes 1048576 | tf_op jit(solution)/shard_map/split | solution.py:53
  175.0 2.4 copy-start.4
  175.9 2.4 copy-start.5
  175.9 2.4 copy-start.6
  187.1 5.4 %copy-start.12 = (bf16[1024,22]{0,1:T(8,128)(2,1)S(1)}, bf16[1024,22]{0,1:T(8,128)(2,1)}, u32[]{:S(2)}) copy-start(bf16[1024,22]{0,1:T(8,128)(2,1)} %param.26) | copy-start | bytes 135172
  187.1 8.8 %all-to-all-start.6 = ((bf16[2,640,1024]{2,1,0:T(8,128)(2,1)}), bf16[2,640,1024]{2,1,0:T(8,128)(2,1)}, u32[]{:S(2)}, u32[]{:S(2)}) async-start(bf16[2,640,1024]{2,1,0:T(8,128)(2,1)} %bitcast.96), calls=%async_computation.6 | async-start | bytes 5242880 | tf_op jit(solution)/shard_map/all_to_all | solution.py:40
  196.6 14.8 %all-to-all-start.3 = ((bf16[2,2048,22]{1,2,0:T(8,128)(2,1)}), bf16[2,2048,22]{1,2,0:T(8,128)(2,1)S(1)}, u32[]{:S(2)}, u32[]{:S(2)}) async-start(bf16[2,2048,22]{1,2,0:T(8,128)(2,1)} %broadcast_in_dim.15), calls=%async_computation.3 | async-start | bytes 393216 | tf_op jit(solution)/shard_map/all_to_all | solution.py:18
  202.4 7.9 %slice-start = ((s8[4718592]{0:T(1024)(128)(4,1)}), s8[524288]{0:T(1024)(128)(4,1)S(1)}, s32[]{:S(2)}) async-start(s8[4718592]{0:T(1024)(128)(4,1)} %bitcast.92), calls=%async_computation.14 | async-start | bytes 1048576
  204.0 6.3 %slice-start.1 = ((s8[4718592]{0:T(1024)(128)(4,1)}), s8[4194304]{0:T(1024)(128)(4,1)S(1)}, s32[]{:S(2)}) async-start(s8[4718592]{0:T(1024)(128)(4,1)} %bitcast.92), calls=%async_computation.15 | async-start | bytes 8388608
  204.0 6.3 %copy-start.13 = (bf16[1024,22]{0,1:T(8,128)(2,1)S(1)}, bf16[1024,22]{0,1:T(8,128)(2,1)}, u32[]{:S(2)}) copy-start(bf16[1024,22]{0,1:T(8,128)(2,1)} %param.27) | copy-start | bytes 135172
  210.2 6.6 %copy-start.7 = (bf16[22,1024]{1,0:T(8,128)(2,1)S(1)}, bf16[22,1024]{1,0:T(8,128)(2,1)}, u32[]{:S(2)}) copy-start(bf16[22,1024]{1,0:T(8,128)(2,1)} %param.28) | copy-start | bytes 135172
  212.2 4.6 %all-to-all-start.4 = ((bf16[2,2048,22]{1,2,0:T(8,128)(2,1)}), bf16[2,2048,22]{1,2,0:T(8,128)(2,1)S(1)}, u32[]{:S(2)}, u32[]{:S(2)}) async-start(bf16[2,2048,22]{1,2,0:T(8,128)(2,1)} %broadcast_in_dim.16), calls=%async_computation.4 | async-start | bytes 393216 | tf_op jit(solution)/shard_map/all_to_all | solution.py:18
  215.6 100.6 %reduce-scatter.4.cloned.1.call-start = ((), (), s32[]{:S(2)}) async-start(), calls=%async_computation.11 | async-start | bytes 9437184 | tf_op jit(solution)/shard_map/reduce_scatter | solution.py:64
  224.7 117.6 %reduce-scatter.6.cloned.1.call-start = ((), (), s32[]{:S(2)}) async-start(), calls=%async_computation.12 | async-start | bytes 1310720 | tf_op jit(solution)/shard_map/reduce_scatter | solution.py:64
  316.3 50.7 %reduce-scatter.8.cloned.1.call-start = ((), (), s32[]{:S(2)}) async-start(), calls=%async_computation.13 | async-start | bytes 327680 | tf_op jit(solution)/shard_map/reduce_scatter | solution.py:64
  (3 other events, 5.0 us)
Sparse Core Ops, SparseCore 0:
  33.8 113.9 all-gather.3
  224.9 91.3 reduce-scatter.3
  318.8 23.5 reduce-scatter.5
  344.7 22.2 reduce-scatter.7
where the time goes:
time: 377 us; the launch traced here: 375 us
  waiting for transfers between devices  227 us (60%)
  blocking collectives  48.7 us (13%)
  matrix products  34 us (9%)
  starting transfers between devices  22.6 us (6%)
  local copies, waits for them, and re-layouts  20.6 us (5%)
  between operations  14.2 us (4%)
  other arithmetic  8.12 us (2%)
    reduce_scatter x3, waiting for transfers between devices, summed_rows(): total = lax.psum_scatter(total, axis, scatter_dimension=0, tiled=True)  142 us
    all_gather x1, waiting for transfers between devices, side_by_side(): filled = lax.all_gather(both, axis, axis=dim, tiled=True)  81.4 us
    all_gather x3, blocking collectives, whole_of(): value = lax.all_gather(value, axis, axis=dim, tiled=True)  34.8 us
    all_to_all x4, starting transfers between devices, copy_for_each(): return lax.all_to_all(copies, axis, split_axis=0, concat_axis=0, tiled=True)  17.1 us
    all_to_all x2, blocking collectives, copy_for_each(): return lax.all_to_all(copies, axis, split_axis=0, concat_axis=0, tiled=True)  13.9 us
    dot_general x1, matrix products, body(): jnp.dot(dense_hidden, dense_down, preferred_element_type=jnp.float32)  7.91 us
  transfers between devices with their start and end apart: 9, of which 7 were waited for; matrix products, arithmetic and copies ran while one was open for 4% of the time, Pallas kernels for 0%

commit v1 on v0

v1 whole, which is shorter than its diff:
```python
import jax
import jax.numpy as jnp
from jax import lax
from jax.experimental import pallas as pl
from jax.experimental.pallas import tpu as pltpu
from jax.sharding import Mesh
from jax.sharding import PartitionSpec as P

EP = ("ep_0", "ep_1", "ep_2")
Z, Y, X = EP
MESH = pl.DeviceIdType.MESH
SLOT = 8
CAP = 5
F32 = jnp.float32
BF16 = jnp.bfloat16
epsilon = 1e-06
COPIES = 120


def iota(shape, dim):
    return lax.broadcasted_iota(jnp.int32, shape, dim)


def dot(a, b):
    return jnp.dot(a, b, preferred_element_type=F32)


def dot_nt(a, b):
    return lax.dot_general(a, b, (((1,), (1,)), ((), ())), preferred_element_type=F32)


def dot_tn(a, b):
    return lax.dot_general(a, b, (((0,), (0,)), ((), ())), preferred_element_type=F32)


def silu(v):
    return v / (1.0 + jnp.exp(-v))


def pack_matrices(c):
    def slots(row, col):
        in_a = (row < 16) & (col == (row // 4) * SLOT + row % 4)
        in_b = (row >= 16) & (row < 20) & (col == (row - 16) * SLOT + 4)
        return jnp.where(in_a | in_b, 1.0, 0.0).astype(BF16)

    def own(row, col):
        return jnp.where((row >= 20) & (row < 28) & (col == c * 8 + row - 20), 1.0, 0.0).astype(BF16)

    return (
        slots(iota((32, 32), 0), iota((32, 32), 1)),
        own(iota((32, 16), 0), iota((32, 16), 1)),
        slots(iota((32, 32), 1), iota((32, 32), 0)),
        own(iota((16, 32), 1), iota((16, 32), 0)),
    )


def kernel(
    tokens,
    norm_mix,
    norm_ffn,
    gate_vec,
    routes,
    route_w,
    dgate,
    dup,
    ddown,
    state,
    w_query,
    w_key,
    w_value,
    w_out,
    egate,
    eup,
    edown,
    mixed,
    new_state,
    wq,
    wk,
    wv,
    wo,
    st,
    read,
    tok_p,
    nf_p,
    gv_p,
    mix_o,
    mix_p,
    we,
    wd,
    disp,
    zrecv,
    xs,
    outs,
    opp_q,
    fin_q,
    tsend,
    opp_p,
    fin_p,
    rbuf,
    ret,
    dsend,
    drecv,
    local_sem,
    send_sem,
    recv_sem,
    ret_send,
    ret_recv,
):
    z, y, x, c = (lax.axis_index(a) for a in (Z, Y, X, "tp"))
    first = c == 0
    size = {Z: 8, Y: 4, X: 4}
    at = {Z: z, Y: y, X: x}
    used = [0]

    def shift(axis, by):
        return {axis: lax.rem(at[axis] + by + size[axis], size[axis])}

    partner = {"tp": 1 - c}

    def remote(src, dst, device):
        n = used[0]
        used[0] += 1
        return pltpu.make_async_remote_copy(
            src_ref=src,
            dst_ref=dst,
            send_sem=send_sem.at[n],
            recv_sem=recv_sem.at[n],
            device_id=device,
            device_id_type=MESH,
        )

    def started(src, dst, device):
        copy = remote(src, dst, device)
        copy.start()
        return copy

    def halves(own, other):
        return jnp.where(first, own, other), jnp.where(first, other, own)

    loads = []
    for n, (src, dst) in enumerate(
        [
            (w_query, wq),
            (w_key, wk),
            (w_value, wv),
            (state, st),
            (w_out, wo),
            (egate, we.at[0, pl.ds(0, 88)]),
            (eup, we.at[1, pl.ds(0, 88)]),
            (edown, we.at[2, pl.ds(0, 88)]),
        ]
    ):
        copy = pltpu.make_async_copy(src, dst, local_sem.at[n])
        copy.start()
        loads.append(copy)

    for t, ref in enumerate((dgate, dup, ddown)):
        block = jnp.concatenate([ref[...].astype(F32), jnp.zeros((2, 1024), F32)], axis=0)
        wd[t, pl.ds(c, 1), pl.ds(0, 24), :] = block.astype(BF16)[None]

    barrier = pltpu.get_barrier_semaphore()
    peers = [partner]
    for by in range(1, 8):
        for core in (c, 1 - c):
            peers.append({**shift(Z, by), "tp": core})
    for axis in (Y, X):
        peers += [shift(axis, 1), shift(axis, -1)]
    for peer in peers:
        pl.semaphore_signal(barrier, inc=1, device_id=peer, device_id_type=MESH)
    pl.semaphore_wait(barrier, len(peers))

    pair = [started(tokens, tok_p, partner), started(norm_ffn, nf_p, partner), started(gate_vec, gv_p, partner)]

    def wd_slot(n):
        return wd.at[:, pl.ds(c, 1), pl.ds(24 * n, 24), :]

    ring = {}
    ring[1] = started(wd_slot(0), wd_slot(1), shift(Z, 1))
    ring[7] = started(wd_slot(0), wd_slot(7), shift(Z, -1))
    swap = [started(src, we.at[t, pl.ds(88, 88)], partner) for t, src in enumerate((egate, eup, edown))]

    for copy in pair:
        copy.wait_recv()
    lo, hi = halves(tokens[...].astype(F32), tok_p[...].astype(F32))
    full = jnp.concatenate([lo, hi], axis=1)
    mean = jnp.sum(full * full, axis=1, keepdims=True) / 2048.0
    normed = (full * lax.rsqrt(mean + epsilon) * norm_mix[...]).astype(BF16)
    for copy in loads[:3]:
        copy.wait()
    query = dot(normed, wq[...]).astype(BF16).astype(F32)
    key = dot(normed, wk[...]).astype(BF16).astype(F32) * 128 ** (-0.5)
    value = dot(normed, wv[...]).astype(BF16).astype(F32)
    blank = jnp.zeros((112, 256), F32)
    query_t = jnp.concatenate([query, blank], axis=0).T
    key_t = jnp.concatenate([key, blank], axis=0).T
    loads[3].wait()
    for h in range(2):
        decay = jnp.where(first, 1.0 - 2.0 ** (-3.0 - 2.0 * h), 1.0 - 2.0 ** (-7.0 - 2.0 * h))
        for s in range(16):
            k_col = key_t[h * 128 : (h + 1) * 128, s : s + 1]
            q_col = query_t[h * 128 : (h + 1) * 128, s : s + 1]
            v_row = value[s : s + 1, h * 128 : (h + 1) * 128]
            new = decay * st[s, h] + k_col * v_row
            st[s, h] = new
            read[s : s + 1, h * 128 : (h + 1) * 128] = jnp.sum(q_col * new, axis=0, keepdims=True)
    keep = pltpu.make_async_copy(st, new_state, local_sem.at[8])
    keep.start()
    heads = []
    for h in range(2):
        part = read[:, h * 128 : (h + 1) * 128]
        centre = jnp.mean(part, axis=1, keepdims=True)
        spread = jnp.mean(jnp.square(part - centre), axis=1, keepdims=True)
        heads.append(((part - centre) * lax.rsqrt(spread + epsilon)).astype(BF16))
    loads[4].wait()
    mix = dot(heads[0], wo[0:128, :]) + dot(heads[1], wo[128:256, :])
    mix_o[...] = mix.astype(BF16)
    mix_copy = started(mix_o, mix_p, partner)

    ring[1].wait_recv()
    ring[2] = started(wd_slot(1), wd_slot(2), shift(Z, 1))
    ring[7].wait_recv()
    ring[6] = started(wd_slot(7), wd_slot(6), shift(Z, -1))

    block = iota((64, 16), 0)
    expert = lax.rem(z - block // SLOT + 8, 8)
    hit0 = jnp.where(routes[0:1, :] == expert, 1.0, 0.0)
    hit1 = jnp.where(routes[1:2, :] == expert, 1.0, 0.0)
    member = hit0 + hit1
    before = jnp.where(iota((16, 16), 0) < iota((16, 16), 1), 1.0, 0.0).astype(BF16)
    place = dot(member.astype(BF16), before)
    chosen = jnp.where(place == (block % SLOT).astype(F32), member, 0.0)
    weights = route_w[...].astype(F32)
    scaled = (chosen * (hit0 * weights[0:1, :] + hit1 * weights[1:2, :])).astype(BF16)
    mine = jnp.where(first, chosen[0:32, :], chosen[32:64, :]).astype(BF16)
    pack_s, pack_o, open_s, open_o = pack_matrices(c)

    mix_copy.wait_recv()
    after = (full + (mix_o[...].astype(F32) + mix_p[...].astype(F32))).astype(BF16).astype(F32)
    mean2 = jnp.sum(after * after, axis=1, keepdims=True) / 2048.0
    nf_lo, nf_hi = halves(norm_ffn[...], nf_p[...])
    normed2 = (after * lax.rsqrt(mean2 + epsilon) * jnp.concatenate([nf_lo, nf_hi], axis=1)).astype(BF16)

    rows = dot(mine, normed2)
    for j in range(4):
        disp[SLOT * j : SLOT * (j + 1), :] = rows[SLOT * j : SLOT * (j + 1), :].astype(BF16)
    sent = []
    for j in range(4):
        part = pl.ds(SLOT * j, SLOT)
        sent.append(remote(disp.at[part], zrecv.at[part], shift(Z, -(4 * c + j))))
    for j in (1, 2, 3):
        sent[j].start()

    @pl.when(first)
    def _():
        zrecv[0:SLOT, :] = disp[0:SLOT, :]

    @pl.when(jnp.logical_not(first))
    def _():
        sent[0].start()

    gv_lo, gv_hi = halves(gate_vec[...].astype(F32), gv_p[...].astype(F32))
    logit = jnp.sum(normed2.astype(F32) * jnp.concatenate([gv_lo, gv_hi], axis=1), axis=1, keepdims=True)
    own_rows = dot(pack_o, normed2)

    for j in (1, 2, 3):
        sent[j].wait_recv()

    @pl.when(jnp.logical_not(first))
    def _():
        sent[0].wait_recv()

    packed = (dot(pack_s, zrecv[...]) + own_rows).astype(BF16)
    xs[0, 0:16, :] = packed[0:16, :]
    xs[1, 0:16, :] = packed[16:32, :]

    axes = ((X, Y), (Y, X))

    def cell(ref, half, rq, rp, part=None):
        base = 16 * (4 * rq + rp)
        start, count = (base, 16) if part is None else (base + 8 * part, 8)
        return ref.at[half, pl.ds(start, count)]

    got = [{}, {}]

    def send_p(half, rp):
        q = axes[half][1]
        got[half][1, rp] = started(cell(xs, half, 0, rp), cell(xs, half, 1, rp), shift(q, 1))
        got[half][3, rp] = started(cell(xs, half, 0, rp), cell(xs, half, 3, rp), shift(q, -1))

    def pass_on(half, rp):
        q = axes[half][1]
        if rp in (0, 2):
            got[half][1, rp].wait_recv()
            got[half][2, rp] = started(cell(xs, half, 1, rp), cell(xs, half, 2, rp), shift(q, 1))
        else:
            got[half][3, rp].wait_recv()
            got[half][2, rp] = started(cell(xs, half, 3, rp), cell(xs, half, 2, rp), shift(q, -1))

    for half in range(2):
        p = axes[half][0]
        got[half][0, 1] = started(cell(xs, half, 0, 0), cell(xs, half, 0, 1), shift(p, 1))
        got[half][0, 3] = started(cell(xs, half, 0, 0), cell(xs, half, 0, 3), shift(p, -1))
    for half in range(2):
        send_p(half, 0)
    across = []
    for half in range(2):
        p = axes[half][0]
        got[half][0, 1].wait_recv()
        across.append(started(cell(xs, half, 0, 1, 0), cell(xs, half, 0, 2, 0), shift(p, 1)))
        send_p(half, 1)
        got[half][0, 3].wait_recv()
        across.append(started(cell(xs, half, 0, 3, 1), cell(xs, half, 0, 2, 1), shift(p, -1)))
        send_p(half, 3)
    ring[2].wait_recv()
    ring[3] = started(wd_slot(2), wd_slot(3), shift(Z, 1))
    ring[6].wait_recv()
    ring[5] = started(wd_slot(6), wd_slot(5), shift(Z, -1))
    for half in range(2):
        pass_on(half, 0)
    for half in range(2):
        across[2 * half].wait_recv()
        across[2 * half + 1].wait_recv()
        send_p(half, 2)
    for half in range(2):
        pass_on(half, 1)
    for half in range(2):
        pass_on(half, 3)
    ring[3].wait_recv()
    ring[4] = started(wd_slot(3), wd_slot(4), shift(Z, 1))
    for half in range(2):
        pass_on(half, 2)
    for half in range(2):
        for rp in (1, 3):
            got[half][1, rp].wait_recv()
        for rp in (0, 2):
            got[half][3, rp].wait_recv()
        for rp in range(4):
            got[half][2, rp].wait_recv()

    for copy in loads[5:]:
        copy.wait()
    for copy in swap:
        copy.wait_recv()

    def expert_hidden(half):
        rows = xs[half]
        return silu(dot_nt(rows, we[0])) * dot_nt(rows, we[1])

    def sum_p(ref, half, rq):
        return ref[half, 64 * rq : 64 * (rq + 1), :]

    hidden = expert_hidden(0).astype(BF16)
    for rq in (2, 1, 3, 0):
        for n in range(4):
            outs[0, 64 * rq : 64 * (rq + 1), 512 * n : 512 * (n + 1)] = dot(
                hidden[64 * rq : 64 * (rq + 1), :], we[2, :, 512 * n : 512 * (n + 1)]
            ).astype(BF16)

    got_q = [{}, {}]

    def reduce_opposite(half):
        q = axes[half][1]
        for rp in range(4):
            device = shift(q, -1 if rp in (0, 2) else 1)
            got_q[half][2, rp] = started(cell(outs, half, 2, rp), opp_q.at[half, pl.ds(16 * rp, 16)], device)

    reduce_opposite(0)

    hidden_e = expert_hidden(1)
    ring[5].wait_recv()
    ring[4].wait_recv()
    whole = started(wd.at[:, pl.ds(c, 1)], wd.at[:, pl.ds(c, 1)], partner)
    place_in = iota((256, 1), 0) % 16
    hidden_e = jnp.where(place_in < 4, hidden_e, 0.0).astype(BF16)
    whole.wait_recv()

    def dense_pre(t):
        return dot_nt(xs[1, :, 0:1024], wd[t, 0]) + dot_nt(xs[1, :, 1024:2048], wd[t, 1])

    hidden_d = jnp.where(place_in >= 4, silu(dense_pre(0)) * dense_pre(1), 0.0).astype(BF16)
    for rq in (2, 1, 3, 0):
        take = slice(64 * rq, 64 * (rq + 1))
        for n in range(4):
            outs[1, take, 512 * n : 512 * (n + 1)] = (
                dot(hidden_e[take, :], we[2, :, 512 * n : 512 * (n + 1)])
                + dot(hidden_d[take, :], wd[2, n // 2, :, 512 * (n % 2) : 512 * (n % 2 + 1)])
            ).astype(BF16)
    reduce_opposite(1)

    def reduce_neighbours(half):
        q = axes[half][1]
        for rp in (0, 2, 1, 3):
            rq, by = (1, -1) if rp in (0, 2) else (3, 1)
            got_q[half][2, rp].wait_recv()
            at_row = 16 * (4 * rq + rp)
            both = outs[half, at_row : at_row + 16, :].astype(F32) + opp_q[half, 16 * rp : 16 * rp + 16, :].astype(F32)
            outs[half, at_row : at_row + 16, :] = both.astype(BF16)
        for rp in range(4):
            for rq, by in ((1, -1), (3, 1)):
                got_q[half][rq, rp] = started(
                    cell(outs, half, rq, rp), fin_q.at[half, rq // 2, pl.ds(16 * rp, 16)], shift(q, by)
                )

    got_p = [{}, {}]

    def reduce_p_start(half):
        p = axes[half][0]
        total = []
        for rp in (2, 1, 3, 0):
            for rq in (1, 3):
                got_q[half][rq, rp].wait_recv()
            take = slice(16 * rp, 16 * rp + 16)
            total.append(
                outs[half, take, :].astype(F32) + fin_q[half, 0, take, :].astype(F32) + fin_q[half, 1, take, :].astype(F32)
            )
            if rp == 2:
                tsend[half, take, :] = total[0].astype(BF16)
                got_p[half]["lo"] = started(
                    tsend.at[half, pl.ds(32, 8)], opp_p.at[half, pl.ds(0, 8)], shift(p, -1)
                )
                got_p[half]["hi"] = started(
                    tsend.at[half, pl.ds(40, 8)], opp_p.at[half, pl.ds(8, 8)], shift(p, 1)
                )
        return total

    def reduce_p_next(half, total):
        p = axes[half][0]
        zero = jnp.zeros((8, 2048), F32)
        got_p[half]["lo"].wait_recv()
        extra = jnp.concatenate([opp_p[half, 0:8, :].astype(F32), zero], axis=0)
        tsend[half, 16:32, :] = (total[1] + extra).astype(BF16)
        got_p[half][1] = started(tsend.at[half, pl.ds(16, 16)], fin_p.at[half, 0], shift(p, -1))
        got_p[half]["hi"].wait_recv()
        extra = jnp.concatenate([zero, opp_p[half, 8:16, :].astype(F32)], axis=0)
        tsend[half, 48:64, :] = (total[2] + extra).astype(BF16)
        got_p[half][3] = started(tsend.at[half, pl.ds(48, 16)], fin_p.at[half, 1], shift(p, 1))

    def reduce_end(half, total):
        got_p[half][1].wait_recv()
        got_p[half][3].wait_recv()
        return total[3] + fin_p[half, 0].astype(F32) + fin_p[half, 1].astype(F32)

    reduce_neighbours(0)
    reduce_neighbours(1)
    totals = [reduce_p_start(0), reduce_p_start(1)]
    for half in range(2):
        reduce_p_next(half, totals[half])
    summed = jnp.concatenate([reduce_end(half, totals[half]) for half in range(2)], axis=0).astype(BF16)

    opened = dot(open_s, summed)
    for h in range(2):
        for j in range(4):
            rbuf[h, SLOT * j : SLOT * (j + 1), :] = opened[
                SLOT * j : SLOT * (j + 1), 1024 * h : 1024 * (h + 1)
            ].astype(BF16)

    def ret_copy(j, h, device):
        d = 4 * c + j
        return pltpu.make_async_remote_copy(
            src_ref=rbuf.at[h, pl.ds(SLOT * j, SLOT)],
            dst_ref=ret.at[pl.ds(pl.multiple_of(SLOT * d, SLOT), SLOT)],
            send_sem=ret_send.at[2 * j + h],
            recv_sem=ret_recv.at[d],
            device_id=device,
            device_id_type=MESH,
        )

    def ret_device(j, h):
        return {**shift(Z, 4 * c + j), "tp": h}

    def ret_each(act):
        for j in (1, 2, 3):
            for h in range(2):
                act(ret_copy(j, h, ret_device(j, h)))

        @pl.when(first)
        def _():
            act(ret_copy(0, 1, {"tp": 1}))

        @pl.when(jnp.logical_not(first))
        def _():
            for h in range(2):
                act(ret_copy(0, h, ret_device(0, h)))

    ret_each(lambda copy: copy.start())

    @pl.when(first)
    def _():
        ret[0:SLOT, :] = rbuf[0, 0:SLOT, :]

    dense_rows = dot(open_o, summed)
    own_half, other_half = halves(dense_rows[:, 0:1024], dense_rows[:, 1024:2048])
    dsend[...] = other_half.astype(BF16)
    dense_copy = started(dsend, drecv, partner)
    after_lo, _ = halves(after[:, 0:1024], after[:, 1024:2048])
    dense_copy.wait_recv()
    dense = (own_half + drecv[...].astype(F32)) * (1.0 / (1.0 + jnp.exp(-logit)))

    def ret_wait(d):
        pltpu.make_async_remote_copy(
            src_ref=rbuf.at[0, pl.ds(0, SLOT)],
            dst_ref=ret.at[pl.ds(SLOT * d, SLOT)],
            send_sem=ret_send.at[0],
            recv_sem=ret_recv.at[d],
            device_id=partner,
            device_id_type=MESH,
        ).wait_recv()

    for d in range(1, 8):
        ret_wait(d)

    @pl.when(jnp.logical_not(first))
    def _():
        ret_wait(0)

    moe = dot_tn(scaled, ret[...])
    mixed[...] = (after_lo + moe + dense).astype(BF16)

    keep.wait()
    for copy in pair + swap + across + [mix_copy, whole, dense_copy]:
        copy.wait_send()
    for group in [ring] + got + got_q + got_p:
        for copy in group.values():
            copy.wait_send()
    for j in (1, 2, 3):
        sent[j].wait_send()

    @pl.when(jnp.logical_not(first))
    def _():
        sent[0].wait_send()

    ret_each(lambda copy: copy.wait_send())
    assert used[0] <= COPIES


def body(
    tokens,
    state,
    norm_mix,
    w_query,
    w_key,
    w_value,
    w_out,
    norm_ffn,
    gate_vector,
    dense_gate,
    dense_up,
    dense_down,
    exp_gate,
    exp_up,
    exp_down,
    routes,
    route_w,
):
    vmem = pl.BlockSpec(memory_space=pltpu.VMEM)
    hbm = pl.BlockSpec(memory_space=pl.ANY)

    def buf(*shape, dtype=BF16):
        return pltpu.VMEM(shape, dtype)

    return pl.pallas_call(
        kernel,
        out_shape=(
            jax.ShapeDtypeStruct(tokens.shape, tokens.dtype),
            jax.ShapeDtypeStruct(state.shape, state.dtype),
        ),
        in_specs=[vmem] * 9 + [hbm] * 8,
        out_specs=(vmem, hbm),
        scratch_shapes=[
            buf(2048, 256),
            buf(2048, 256),
            buf(2048, 256),
            buf(256, 2048),
            buf(16, 2, 128, 128, dtype=F32),
            buf(16, 256, dtype=F32),
            buf(16, 1024),
            buf(1, 1024, dtype=F32),
            buf(1, 1024),
            buf(16, 2048),
            buf(16, 2048),
            buf(3, 176, 2048),
            buf(3, 2, 192, 1024),
            buf(32, 2048),
            buf(32, 2048),
            buf(2, 256, 2048),
            buf(2, 256, 2048),
            buf(2, 64, 2048),
            buf(2, 2, 64, 2048),
            buf(2, 64, 2048),
            buf(2, 16, 2048),
            buf(2, 2, 16, 2048),
            buf(2, 32, 1024),
            buf(64, 1024),
            buf(16, 1024),
            buf(16, 1024),
            pltpu.SemaphoreType.DMA((9,)),
            pltpu.SemaphoreType.DMA((COPIES,)),
            pltpu.SemaphoreType.DMA((COPIES,)),
            pltpu.SemaphoreType.DMA((8,)),
            pltpu.SemaphoreType.DMA((8,)),
        ],
        compiler_params=pltpu.CompilerParams(
            collective_id=0, has_side_effects=True, vmem_limit_bytes=48 * 1024 * 1024
        ),
        name="layer",
    )(
        tokens,
        norm_mix.reshape(1, -1),
        norm_ffn.reshape(1, -1),
        gate_vector.reshape(1, -1),
        routes.T,
        route_w.T,
        dense_gate.T,
        dense_up.T,
        dense_down,
        state,
        w_query,
        w_key,
        w_value,
        w_out,
        exp_gate[0].T,
        exp_up[0].T,
        exp_down[0],
    )


def solution(mesh):
    finer = Mesh(mesh.devices.reshape(8, 4, 4, mesh.shape["tp"]), (*EP, "tp"))
    in_specs = (
        P(EP, "tp"),
        P(EP, "tp", None, None),
        P(),
        P(None, "tp"),
        P(None, "tp"),
        P(None, "tp"),
        P("tp", None),
        P("tp"),
        P("tp"),
        P("tp", EP),
        P("tp", EP),
        P(EP, "tp"),
        P(EP, None, "tp"),
        P(EP, None, "tp"),
        P(EP, "tp", None),
        P(EP, None),
        P(EP, None),
    )
    out_specs = (P(EP, "tp"), P(EP, "tp", None, None))
    return jax.shard_map(body, mesh=finer, in_specs=in_specs, out_specs=out_specs, check_vma=False)
```

time: 377 us -> 93.5 us (0.25)
  waiting for transfers between devices: 227 us -> 0 us
  Pallas kernels: 0 us -> 73.9 us
  blocking collectives: 48.7 us -> 0 us
  matrix products: 34 us -> 0 us
  starting transfers between devices: 22.6 us -> 0 us
  between operations: 14.2 us -> 0.65 us
  other arithmetic: 8.12 us -> 0 us
    reduce_scatter x3 -> x0, waiting for transfers between devices: 142 us -> none  [summed_rows(): total = lax.psum_scatter(total, axis, scatter_dimension=0, tiled=True)]
    all_gather x1 -> x0, waiting for transfers between devices: 81.4 us -> none  [side_by_side(): filled = lax.all_gather(both, axis, axis=dim, tiled=True)]
    pallas_call x0 -> x1, Pallas kernels: none -> 73.9 us  [body(): pl.pallas_call(kernel, out_shape=(jax.ShapeDtypeStruct(tokens.shape, toke...]
    all_gather x3 -> x0, blocking collectives: 34.8 us -> none  [whole_of(): value = lax.all_gather(value, axis, axis=dim, tiled=True)]
    dot_general x13 -> x0, matrix products: 34 us -> none  [the longest x1 7.91 us: body(): jnp.dot(dense_hidden, dense_down, preferred_element_type=jnp.float32)]
    all_to_all x5 -> x0, starting transfers between devices: 22.5 us -> none  [the longest x4 17.1 us: copy_for_each(): return lax.all_to_all(copies, axis, split_axis=0, concat_axis=0, tiled=True)]
    all_to_all x2 -> x0, blocking collectives: 13.9 us -> none  [copy_for_each(): return lax.all_to_all(copies, axis, split_axis=0, concat_axis=0, tiled=True)]
    unnamed x39 -> x32, local copies, waits for them, and re-layouts: 4 us -> 17.5 us
  transfers between devices with their start and end apart: 9 -> 0, of which waited for: 7 -> 0; matrix products, arithmetic and copies ran while one was open for 4% -> 0% of each run, Pallas kernels for 0% -> 0%
where the time goes in v1:
time: 93.5 us; the launch traced here: 92.7 us
  Pallas kernels  73.9 us (79%)
  local copies, waits for them, and re-layouts  18.2 us (19%)
    pallas_call x1, Pallas kernels, body(): pl.pallas_call(kernel, out_shape=(jax.ShapeDtypeStruct(tokens.shape, toke...  73.9 us
    unnamed x32, local copies, waits for them, and re-layouts  17.5 us

profile of v1, /device:TPU:1, one launch (start us, length us, event | category | flops | bytes accessed | tf_op | source)
XLA Modules:
  0.0 92.7 jit_solution(15572493907334696390)
XLA Ops:
  0.6 0.7 reshape.15.gate_vec
  1.3 0.0 copy-start
  1.3 1.2 %copy-done = bf16[2048,256]{1,0:T(8,128)(2,1)S(1)} copy-done((bf16[2048,256]{1,0:T(8,128)(2,1)S(1)}, bf16[2048,256]{1,0:T(8,128)(2,1)}, u32[]{:S(2)}) %copy-start) | copy-done | bytes 1048600
  2.5 0.0 copy-start.1
  2.5 1.2 %copy-done.1 = bf16[2048,256]{1,0:T(8,128)(2,1)S(1)} copy-done((bf16[2048,256]{1,0:T(8,128)(2,1)S(1)}, bf16[2048,256]{1,0:T(8,128)(2,1)}, u32[]{:S(2)}) %copy-start.1) | copy-done | bytes 1048600
  3.8 0.0 copy-start.2
  3.8 1.2 %copy-done.2 = bf16[2048,256]{1,0:T(8,128)(2,1)S(1)} copy-done((bf16[2048,256]{1,0:T(8,128)(2,1)S(1)}, bf16[2048,256]{1,0:T(8,128)(2,1)}, u32[]{:S(2)}) %copy-start.2) | copy-done | bytes 1048600
  5.0 0.0 copy-start.3
  5.0 1.2 %copy-done.3 = bf16[256,2048]{1,0:T(8,128)(2,1)S(1)} copy-done((bf16[256,2048]{1,0:T(8,128)(2,1)S(1)}, bf16[256,2048]{1,0:T(8,128)(2,1)}, u32[]{:S(2)}) %copy-start.3) | copy-done | bytes 1048600
  6.2 0.0 copy-start.4
  6.2 1.0 %copy-done.4 = bf16[1,2048,88]{1,2,0:T(8,128)(2,1)S(1)} copy-done((bf16[1,2048,88]{1,2,0:T(8,128)(2,1)S(1)}, bf16[1,2048,88]{1,2,0:T(8,128)(2,1)}, u32[]{:S(2)}) %copy-start.4) | copy-done | bytes 360472
  7.2 1.0 %copy-done.5 = bf16[1,2048,88]{1,2,0:T(8,128)(2,1)S(1)} copy-done((bf16[1,2048,88]{1,2,0:T(8,128)(2,1)S(1)}, bf16[1,2048,88]{1,2,0:T(8,128)(2,1)}, u32[]{:S(2)}) %copy-start.5) | copy-done | bytes 360472
  8.2 1.0 %copy-done.6 = bf16[1,88,2048]{2,1,0:T(8,128)(2,1)S(1)} copy-done((bf16[1,88,2048]{2,1,0:T(8,128)(2,1)S(1)}, bf16[1,88,2048]{2,1,0:T(8,128)(2,1)}, u32[]{:S(2)}) %copy-start.6) | copy-done | bytes 360472
  9.2 0.8 copy-done.7
  10.0 0.8 copy-done.8
  10.8 0.8 copy-done.9
  11.6 0.8 copy-done.10
  12.3 0.7 copy-done.11
  13.0 0.7 copy-done.12
  13.7 0.7 copy-done.13
  14.4 0.7 copy-done.14
  15.0 73.9 %layer.1 = (bf16[16,1024]{1,0:T(8,128)(2,1)S(1)}, f32[16,2,128,128]{3,2,1,0:T(8,128)}) custom-call(bf16[16,1024]{1,0:T(8,128)(2,1)S(1)} %copy-done.10, f32[1,2048]{1,0:T(1,128)S(1)} %bitcast.18, f32[1,1024]{1,0:T(1,128)S(1)} %bitcast.19, bf16[1,1024]{1,0:T(2,128)(2,1)S(1)} %reshape.15.gate_vec, s32[2,16]{1,0:T(2,128)S(1)} %bitcast.20, ...), custom_call_target="tpu_custom_call" | custom-call | tf_op jit(solution)/shard_map/layer/pallas_call | solution.py:561
  89.0 0.6 copy.21
  89.6 3.1 %copy.22 = f32[16,2,128,128]{3,2,1,0:T(8,128)} copy(f32[16,2,128,128]{3,2,1,0:T(8,128)} %get-tuple-element.5) | data formatting | bytes 4194304
  (10 shorter events, 0.0 us)
Async XLA Ops:
  1.3 1.2 %copy-start = (bf16[2048,256]{1,0:T(8,128)(2,1)S(1)}, bf16[2048,256]{1,0:T(8,128)(2,1)}, u32[]{:S(2)}) copy-start(bf16[2048,256]{1,0:T(8,128)(2,1)} %w_query.1) | copy-start | bytes 3145732
  2.5 1.2 %copy-start.1 = (bf16[2048,256]{1,0:T(8,128)(2,1)S(1)}, bf16[2048,256]{1,0:T(8,128)(2,1)}, u32[]{:S(2)}) copy-start(bf16[2048,256]{1,0:T(8,128)(2,1)} %w_key.1) | copy-start | bytes 3145732
  3.8 1.2 %copy-start.2 = (bf16[2048,256]{1,0:T(8,128)(2,1)S(1)}, bf16[2048,256]{1,0:T(8,128)(2,1)}, u32[]{:S(2)}) copy-start(bf16[2048,256]{1,0:T(8,128)(2,1)} %w_value.1) | copy-start | bytes 3145732
  5.0 1.2 %copy-start.3 = (bf16[256,2048]{1,0:T(8,128)(2,1)S(1)}, bf16[256,2048]{1,0:T(8,128)(2,1)}, u32[]{:S(2)}) copy-start(bf16[256,2048]{1,0:T(8,128)(2,1)} %w_out.1) | copy-start | bytes 3145732
  6.2 1.0 %copy-start.4 = (bf16[1,2048,88]{1,2,0:T(8,128)(2,1)S(1)}, bf16[1,2048,88]{1,2,0:T(8,128)(2,1)}, u32[]{:S(2)}) copy-start(bf16[1,2048,88]{1,2,0:T(8,128)(2,1)} %param.29) | copy-start | bytes 1081348
  7.2 1.0 %copy-start.5 = (bf16[1,2048,88]{1,2,0:T(8,128)(2,1)S(1)}, bf16[1,2048,88]{1,2,0:T(8,128)(2,1)}, u32[]{:S(2)}) copy-start(bf16[1,2048,88]{1,2,0:T(8,128)(2,1)} %param.30) | copy-start | bytes 1081348
  8.2 1.0 %copy-start.6 = (bf16[1,88,2048]{2,1,0:T(8,128)(2,1)S(1)}, bf16[1,88,2048]{2,1,0:T(8,128)(2,1)}, u32[]{:S(2)}) copy-start(bf16[1,88,2048]{2,1,0:T(8,128)(2,1)} %param.31) | copy-start | bytes 1081348
  9.2 0.8 copy-start.7
  10.0 0.8 copy-start.8
  10.8 0.8 copy-start.9
  11.6 0.8 copy-start.10
  12.3 0.7 copy-start.11
  13.0 0.7 copy-start.12
  13.7 0.7 copy-start.13
  14.4 0.7 copy-start.14

commit v2 on v1

v2 whole, which is shorter than its diff:
```python
import jax
import jax.numpy as jnp
from jax import lax
from jax.experimental import pallas as pl
from jax.experimental.pallas import tpu as pltpu
from jax.sharding import Mesh
from jax.sharding import PartitionSpec as P

EP = ("ep_0", "ep_1", "ep_2")
Z, Y, X = EP
MESH = pl.DeviceIdType.MESH
SLOT = 8
CAP = 5
F32 = jnp.float32
BF16 = jnp.bfloat16
epsilon = 1e-06
COPIES = 80
AT = {2: 0, 1: 1, 3: 2, 0: 3}
PASS = {0: -1, 1: 1, 3: -1}


def iota(shape, dim):
    return lax.broadcasted_iota(jnp.int32, shape, dim)


def dot(a, b):
    return jnp.dot(a, b, preferred_element_type=F32)


def dot_nt(a, b):
    return lax.dot_general(a, b, (((1,), (1,)), ((), ())), preferred_element_type=F32)


def dot_tn(a, b):
    return lax.dot_general(a, b, (((0,), (0,)), ((), ())), preferred_element_type=F32)


def silu(v):
    return v / (1.0 + jnp.exp(-v))


def pack_matrix(row, col):
    return jnp.where((row < 4 * CAP) & (col == row // CAP * SLOT + row % CAP), 1.0, 0.0).astype(BF16)


def kernel(
    tokens_h,
    norm_mix_h,
    norm_ffn_h,
    gate_vec_h,
    routes_h,
    route_w_h,
    dgate_h,
    dup_h,
    ddown_h,
    state,
    w_query,
    w_key,
    w_value,
    w_out,
    egate,
    eup,
    edown,
    mixed,
    key_out,
    value_out,
    tokens,
    norm_mix,
    norm_ffn,
    gate_vec,
    routes,
    route_w,
    dgate,
    dup,
    ddown,
    wq,
    wk,
    wv,
    wo,
    st,
    read,
    tok_p,
    nf_p,
    mix_o,
    mix_p,
    we,
    wd,
    disp,
    zrecv,
    xs,
    outs,
    opp_q,
    fin_q,
    tsend,
    fin_p,
    rbuf,
    ret,
    local_sem,
    send_sem,
    recv_sem,
    ret_send,
    ret_recv,
):
    z, y, x, c = (lax.axis_index(a) for a in (Z, Y, X, "tp"))
    first = c == 0
    used = [0]

    def wrap(value, size):
        return lax.rem(value + size, size)

    def along_z(by):
        return {Z: wrap(z + by, 8)}

    def along_p(by):
        return {X: wrap(x + by * (1 - c), 4), Y: wrap(y + by * c, 4)}

    def along_q(by):
        return {X: wrap(x + by * c, 4), Y: wrap(y + by * (1 - c), 4)}

    partner = {"tp": 1 - c}

    def remote(src, dst, device):
        n = used[0]
        used[0] += 1
        return pltpu.make_async_remote_copy(
            src_ref=src,
            dst_ref=dst,
            send_sem=send_sem.at[n],
            recv_sem=recv_sem.at[n],
            device_id=device,
            device_id_type=MESH,
        )

    sent = []

    def started(src, dst, device):
        copy = remote(src, dst, device)
        copy.start()
        sent.append(copy)
        return copy

    def halves(own, other):
        return jnp.where(first, own, other), jnp.where(first, other, own)

    def as_row(ref):
        rows = ref[...].astype(F32)
        return jnp.concatenate([rows[i : i + 1, :] for i in range(8)], axis=1)

    loads = {}
    for n, (src, dst) in enumerate(
        [
            (tokens_h, tokens),
            (norm_ffn_h, norm_ffn),
            (dgate_h, dgate),
            (dup_h, dup),
            (ddown_h, ddown),
            (gate_vec_h, gate_vec),
            (norm_mix_h, norm_mix),
            (routes_h, routes),
            (route_w_h, route_w),
            (w_query, wq),
            (w_key, wk),
            (w_value, wv),
            (state, st),
            (w_out, wo),
            (egate, we.at[0, pl.ds(0, 88)]),
            (eup, we.at[1, pl.ds(0, 88)]),
            (edown, we.at[2, pl.ds(0, 88)]),
        ]
    ):
        loads[n] = pltpu.make_async_copy(src, dst, local_sem.at[n])
        loads[n].start()

    barrier = pltpu.get_barrier_semaphore()
    peers = [partner]
    for by in range(1, 8):
        for core in (c, 1 - c):
            peers.append({**along_z(by), "tp": core})
    for by in (1, -1, 2):
        peers += [along_p(by), along_q(by)]
    for peer in peers:
        pl.semaphore_signal(barrier, inc=1, device_id=peer, device_id_type=MESH)

    for n in range(9):
        loads[n].wait()
    tail = jnp.zeros((2, 1024), F32)
    gate_tail = jnp.concatenate([as_row(gate_vec), tail[0:1, :]], axis=0)
    for t, (ref, end) in enumerate(((dgate, gate_tail), (dup, tail), (ddown, tail))):
        block = jnp.concatenate([ref[...].astype(F32), end], axis=0)
        wd[t, pl.ds(c, 1), pl.ds(0, 24), :] = block.astype(BF16)[None]

    pl.semaphore_wait(barrier, len(peers))

    pair = [started(tokens, tok_p, partner), started(norm_ffn, nf_p, partner)]

    def wd_slot(n):
        return wd.at[:, pl.ds(c, 1), pl.ds(24 * n, 24), :]

    ring, cross = {}, {}

    def forward(source, target):
        ring[target] = started(wd_slot(source), wd_slot(target), along_z(1 if target < 5 else -1))

    def last(source, start, count, by):
        def part(n):
            return wd.at[pl.ds(start, count), pl.ds(c, 1), pl.ds(24 * n, 24), :]

        ring[4, by] = started(part(source), part(4), along_z(by))

    def across(n):
        cross[n] = started(wd_slot(n), wd_slot(n), partner)

    forward(0, 1)
    forward(0, 7)
    swap = [started(src, we.at[t, pl.ds(88, 88)], partner) for t, src in enumerate((egate, eup, edown))]
    across(0)

    for copy in pair:
        copy.wait_recv()
    lo, hi = halves(tokens[...].astype(F32), tok_p[...].astype(F32))
    full = jnp.concatenate([lo, hi], axis=1)
    mean = jnp.sum(full * full, axis=1, keepdims=True) / 2048.0
    normed = (full * lax.rsqrt(mean + epsilon) * norm_mix[...]).astype(BF16)
    for n in (9, 10, 11):
        loads[n].wait()
    query = dot(normed, wq[...]).astype(BF16).astype(F32)
    key = dot(normed, wk[...]).astype(BF16).astype(F32) * 128 ** (-0.5)
    value = dot(normed, wv[...]).astype(BF16).astype(F32)
    key_out[...] = key
    value_out[...] = value
    blank = jnp.zeros((112, 256), F32)
    query_t = jnp.concatenate([query, blank], axis=0).T
    key_t = jnp.concatenate([key, blank], axis=0).T
    loads[12].wait()
    for h in range(2):
        decay = jnp.where(first, 1.0 - 2.0 ** (-3.0 - 2.0 * h), 1.0 - 2.0 ** (-7.0 - 2.0 * h))
        for s in range(16):
            k_col = key_t[h * 128 : (h + 1) * 128, s : s + 1]
            q_col = query_t[h * 128 : (h + 1) * 128, s : s + 1]
            v_row = value[s : s + 1, h * 128 : (h + 1) * 128]
            new = decay * st[s, h] + k_col * v_row
            read[s : s + 1, h * 128 : (h + 1) * 128] = jnp.sum(q_col * new, axis=0, keepdims=True)
    heads = []
    for h in range(2):
        part = read[:, h * 128 : (h + 1) * 128]
        centre = jnp.mean(part, axis=1, keepdims=True)
        spread = jnp.mean(jnp.square(part - centre), axis=1, keepdims=True)
        heads.append(((part - centre) * lax.rsqrt(spread + epsilon)).astype(BF16))
    loads[13].wait()
    mix = dot(heads[0], wo[0:128, :]) + dot(heads[1], wo[128:256, :])
    mix_o[...] = mix.astype(BF16)
    mix_copy = started(mix_o, mix_p, partner)

    block = iota((64, 16), 0)
    expert = lax.rem(z - block // SLOT + 8, 8)
    hit0 = jnp.where(routes[0:1, :] == expert, 1.0, 0.0)
    hit1 = jnp.where(routes[1:2, :] == expert, 1.0, 0.0)
    member = hit0 + hit1
    before = jnp.where(iota((16, 16), 0) < iota((16, 16), 1), 1.0, 0.0).astype(BF16)
    place = dot(member.astype(BF16), before)
    chosen = jnp.where(place == (block % SLOT).astype(F32), member, 0.0)
    weights = route_w[...].astype(F32)
    slot_w = jnp.sum(chosen * (hit0 * weights[0:1, :] + hit1 * weights[1:2, :]), axis=1, keepdims=True)
    slot_first = jnp.sum(chosen * hit0, axis=1, keepdims=True)
    lane = iota((64, 128), 1)
    extra = jnp.where(lane == 0, slot_w, jnp.where(lane == 1, slot_first, 0.0))
    extra = jnp.where(first, extra[0:32, :], extra[32:64, :]).astype(BF16)
    mine = jnp.where(first, chosen[0:32, :], chosen[32:64, :]).astype(BF16)

    mix_copy.wait_recv()
    after = (full + (mix_o[...].astype(F32) + mix_p[...].astype(F32))).astype(BF16).astype(F32)
    mean2 = jnp.sum(after * after, axis=1, keepdims=True) / 2048.0
    nf_lo, nf_hi = halves(norm_ffn[...], nf_p[...])
    normed2 = (after * lax.rsqrt(mean2 + epsilon) * jnp.concatenate([nf_lo, nf_hi], axis=1)).astype(BF16)

    rows = dot(mine, normed2)
    disp[:, 2048:2176] = extra
    disp[:, 0:2048] = rows.astype(BF16)
    moved = []
    for j in range(4):
        part = pl.ds(SLOT * j, SLOT)
        moved.append(remote(disp.at[part], zrecv.at[part], along_z(-(4 * c + j))))
    for j in (3, 2, 1):
        moved[j].start()

    @pl.when(first)
    def _():
        zrecv[0:SLOT, :] = disp[0:SLOT, :]

    @pl.when(jnp.logical_not(first))
    def _():
        moved[0].start()

    ring[1].wait_recv()
    forward(1, 2)
    ring[7].wait_recv()
    forward(7, 6)
    across(1)
    across(7)

    for j in (1, 2, 3):
        moved[j].wait_recv()

    @pl.when(jnp.logical_not(first))
    def _():
        moved[0].wait_recv()

    def cell(ref, rq, rp, start=0, count=24):
        return ref.at[pl.ds(24 * (4 * AT[rq] + rp) + start, count)]

    def cell_rows(ref, rq, rp):
        base = 24 * (4 * AT[rq] + rp)
        return ref[base : base + 24, :].astype(F32)

    def set_rows(ref, rq, rp, rows):
        base = 24 * (4 * AT[rq] + rp)
        ref[base : base + 24, :] = rows.astype(BF16)

    set_rows(xs, 0, 0, dot(pack_matrix(iota((24, 32), 0), iota((24, 32), 1)), zrecv[...]))

    got = {}

    def send_q(rp):
        got[1, rp] = started(cell(xs, 0, rp), cell(xs, 1, rp), along_q(1))
        got[3, rp] = started(cell(xs, 0, rp), cell(xs, 3, rp), along_q(-1))

    def pass_on(rp):
        by = PASS[rp]
        near = 2 - by
        got[near, rp].wait_recv()
        got[2, rp] = started(cell(xs, near, rp), cell(xs, 2, rp), along_q(by))

    got[0, 1] = started(cell(xs, 0, 0), cell(xs, 0, 1), along_p(1))
    got[0, 3] = started(cell(xs, 0, 0), cell(xs, 0, 3), along_p(-1))
    got[0, 2] = started(cell(xs, 0, 0), cell(xs, 0, 2), along_p(2))
    send_q(0)
    got[0, 1].wait_recv()
    send_q(1)
    got[0, 3].wait_recv()
    send_q(3)
    pass_on(0)
    ring[2].wait_recv()
    forward(2, 3)
    ring[6].wait_recv()
    forward(6, 5)
    across(2)
    across(6)
    got[0, 2].wait_recv()
    send_q(2)
    got[2, 2] = started(cell(xs, 0, 2), cell(xs, 2, 2), along_q(2))
    pass_on(1)
    pass_on(3)
    ring[3].wait_recv()
    last(3, 0, 2, 1)
    across(3)
    ring[5].wait_recv()
    last(5, 2, 1, -1)
    across(5)
    for rp in range(4):
        for rq in (1, 3):
            if rp == 2 or PASS[rp] != 2 - rq:
                got[rq, rp].wait_recv()

    for n in (14, 15, 16):
        loads[n].wait()
    for copy in swap:
        copy.wait_recv()

    def hidden_rows(start, count):
        rows = xs[start : start + count, 0:2048]
        scale = xs[start : start + count, 2048:2049].astype(F32)
        return (silu(dot_nt(rows, we[0])) * dot_nt(rows, we[1]) * scale).astype(BF16)

    hidden_near = hidden_rows(96, 288)
    for rp in range(4):
        got[2, rp].wait_recv()
    hidden_far = hidden_rows(0, 96)

    ring[4, 1].wait_recv()
    ring[4, -1].wait_recv()
    across(4)
    for n in range(8):
        cross[n].wait_recv()

    def dense_pre(t):
        return dot_nt(xs[:, 0:1024], wd[t, 0]) + dot_nt(xs[:, 1024:2048], wd[t, 1])

    pre = dense_pre(0)
    dense_scale = xs[:, 2049:2050].astype(F32) / (1.0 + jnp.exp(-pre[:, 22:23]))
    hidden_d = (silu(pre) * dense_pre(1) * dense_scale).astype(BF16)

    def down(hidden_e, start, count):
        take = slice(start, start + count)
        for n in range(4):
            outs[take, 512 * n : 512 * (n + 1)] = (
                dot(hidden_e, we[2, :, 512 * n : 512 * (n + 1)])
                + dot(hidden_d[take, :], wd[2, n // 2, :, 512 * (n % 2) : 512 * (n % 2 + 1)])
            ).astype(BF16)

    back = {}

    def at_rp(ref, rp):
        return ref.at[pl.ds(24 * rp, 24)]

    def rp_rows(ref, rp):
        return ref[24 * rp : 24 * rp + 24, :].astype(F32)

    down(hidden_far, 0, 96)
    direct = started(cell(outs, 2, 2), at_rp(opp_q, 2), along_q(2))
    for rp in (1, 3, 0):
        back[2, rp] = started(cell(outs, 2, rp), at_rp(opp_q, rp), along_q(-PASS[rp]))
    down(hidden_near, 96, 288)

    def send_back(rq, rp):
        back[rq, rp] = started(cell(outs, rq, rp), at_rp(fin_q.at[rq // 2], rp), along_q(-1 if rq == 1 else 1))

    for rq, rp in ((1, 2), (3, 2), (1, 1), (3, 1), (1, 3), (3, 3), (1, 0), (3, 0)):
        if rp == 2 or PASS[rp] != 2 - rq:
            send_back(rq, rp)
    for rp in (1, 3, 0):
        rq = 2 - PASS[rp]
        back[2, rp].wait_recv()
        set_rows(outs, rq, rp, cell_rows(outs, rq, rp) + rp_rows(opp_q, rp))
        send_back(rq, rp)

    total = {}

    def sum_q(rp):
        for rq in (1, 3):
            back[rq, rp].wait_recv()
        total[rp] = cell_rows(outs, 0, rp) + rp_rows(fin_q.at[0], rp) + rp_rows(fin_q.at[1], rp)

    def send_p(n, rp, by):
        rows = pl.ds(24 * n, 24)
        tsend[24 * n : 24 * n + 24, :] = total[rp].astype(BF16)
        back["p", n] = started(tsend.at[rows], fin_p.at[rows], along_p(by))

    sum_q(2)
    direct.wait_recv()
    total[2] = total[2] + rp_rows(opp_q, 2)
    send_p(0, 2, 2)
    sum_q(1)
    send_p(1, 1, -1)
    sum_q(3)
    send_p(2, 3, 1)
    sum_q(0)
    for n in range(3):
        back["p", n].wait_recv()
    summed = (total[0] + rp_rows(fin_p, 0) + rp_rows(fin_p, 1) + rp_rows(fin_p, 2)).astype(BF16)

    opened = dot(pack_matrix(iota((32, 24), 1), iota((32, 24), 0)), summed)
    for h in range(2):
        rbuf[h] = opened[:, 1024 * h : 1024 * (h + 1)].astype(BF16)

    def ret_copy(j, h, device):
        d = 4 * c + j
        return pltpu.make_async_remote_copy(
            src_ref=rbuf.at[h, pl.ds(SLOT * j, SLOT)],
            dst_ref=ret.at[pl.ds(pl.multiple_of(SLOT * d, SLOT), SLOT)],
            send_sem=ret_send.at[2 * j + h],
            recv_sem=ret_recv.at[d],
            device_id=device,
            device_id_type=MESH,
        )

    def ret_device(j, h):
        return {**along_z(4 * c + j), "tp": h}

    def ret_each(act):
        for j in (3, 2, 1):
            for h in range(2):
                act(ret_copy(j, h, ret_device(j, h)))

        @pl.when(first)
        def _():
            act(ret_copy(0, 1, {"tp": 1}))

        @pl.when(jnp.logical_not(first))
        def _():
            for h in range(2):
                act(ret_copy(0, h, ret_device(0, h)))

    ret_each(lambda copy: copy.start())

    @pl.when(first)
    def _():
        ret[0:SLOT, :] = rbuf[0, 0:SLOT, :]

    def ret_wait(d):
        pltpu.make_async_remote_copy(
            src_ref=rbuf.at[0, pl.ds(0, SLOT)],
            dst_ref=ret.at[pl.ds(SLOT * d, SLOT)],
            send_sem=ret_send.at[0],
            recv_sem=ret_recv.at[d],
            device_id=partner,
            device_id_type=MESH,
        ).wait_recv()

    after_own, _ = halves(after[:, 0:1024], after[:, 1024:2048])
    for d in range(1, 8):
        ret_wait(d)

    @pl.when(jnp.logical_not(first))
    def _():
        ret_wait(0)

    mixed[...] = after_own + dot_tn(chosen.astype(BF16), ret[...])

    for copy in sent:
        copy.wait_send()
    for j in (1, 2, 3):
        moved[j].wait_send()

    @pl.when(jnp.logical_not(first))
    def _():
        moved[0].wait_send()

    ret_each(lambda copy: copy.wait_send())
    assert used[0] <= COPIES


def finish(summed_h, key_h, value_h, state_h, mixed_h, new_h, summed, key, value, mixed, st, sem, in_sem, out_sem):
    small = [
        pltpu.make_async_copy(src, dst, sem.at[n])
        for n, (src, dst) in enumerate(((key_h, key), (value_h, value), (summed_h, summed)))
    ]
    for copy in small:
        copy.start()
    pieces = []
    for n in range(8):
        part = pl.ds(2 * n, 2)
        pieces.append(pltpu.make_async_copy(state_h.at[part], st.at[part], in_sem.at[n]))
        pieces[n].start()
    for copy in small:
        copy.wait()
    mixed[...] = summed[...].astype(BF16)
    stores = [pltpu.make_async_copy(mixed, mixed_h, out_sem.at[8])]
    stores[0].start()
    key_t = jnp.concatenate([key[...], jnp.zeros((112, 256), F32)], axis=0).T
    first = lax.axis_index("tp") == 0
    decay = [jnp.where(first, 1.0 - 2.0 ** (-3.0 - 2.0 * h), 1.0 - 2.0 ** (-7.0 - 2.0 * h)) for h in range(2)]
    for n in range(8):
        pieces[n].wait()
        for s in (2 * n, 2 * n + 1):
            for h in range(2):
                span = slice(128 * h, 128 * h + 128)
                st[s, h] = decay[h] * st[s, h] + key_t[span, s : s + 1] * value[s : s + 1, span]
        part = pl.ds(2 * n, 2)
        stores.append(pltpu.make_async_copy(st.at[part], new_h.at[part], out_sem.at[n]))
        stores[-1].start()
    for copy in stores:
        copy.wait()


def body(
    tokens,
    state,
    norm_mix,
    w_query,
    w_key,
    w_value,
    w_out,
    norm_ffn,
    gate_vector,
    dense_gate,
    dense_up,
    dense_down,
    exp_gate,
    exp_up,
    exp_down,
    routes,
    route_w,
):
    vmem = pl.BlockSpec(memory_space=pltpu.VMEM)
    hbm = pl.BlockSpec(memory_space=pltpu.HBM)

    def buf(*shape, dtype=BF16):
        return pltpu.VMEM(shape, dtype)

    summed, key, value = pl.pallas_call(
        kernel,
        out_shape=(
            jax.ShapeDtypeStruct(tokens.shape, F32),
            jax.ShapeDtypeStruct((16, 256), F32),
            jax.ShapeDtypeStruct((16, 256), F32),
        ),
        in_specs=[hbm] * 17,
        out_specs=(vmem, vmem, vmem),
        scratch_shapes=[
            buf(16, 1024),
            buf(1, 2048, dtype=F32),
            buf(1, 1024, dtype=F32),
            buf(8, 128),
            buf(2, 16, dtype=jnp.int32),
            buf(2, 16),
            buf(22, 1024),
            buf(22, 1024),
            buf(22, 1024),
            buf(2048, 256),
            buf(2048, 256),
            buf(2048, 256),
            buf(256, 2048),
            buf(16, 2, 128, 128, dtype=F32),
            buf(16, 256, dtype=F32),
            buf(16, 1024),
            buf(1, 1024, dtype=F32),
            buf(16, 2048),
            buf(16, 2048),
            buf(3, 176, 2048),
            buf(3, 2, 192, 1024),
            buf(32, 2176),
            buf(32, 2176),
            buf(384, 2176),
            buf(384, 2048),
            buf(96, 2048),
            buf(2, 96, 2048),
            buf(72, 2048),
            buf(72, 2048),
            buf(2, 32, 1024),
            buf(64, 1024),
            pltpu.SemaphoreType.DMA((17,)),
            pltpu.SemaphoreType.DMA((COPIES,)),
            pltpu.SemaphoreType.DMA((COPIES,)),
            pltpu.SemaphoreType.DMA((8,)),
            pltpu.SemaphoreType.DMA((8,)),
        ],
        compiler_params=pltpu.CompilerParams(collective_id=0, has_side_effects=True, vmem_limit_bytes=67043328),
        name="layer",
    )(
        tokens,
        norm_mix.reshape(1, -1),
        norm_ffn.reshape(1, -1),
        gate_vector.reshape(8, 128),
        routes.T,
        route_w.T,
        dense_gate.T,
        dense_up.T,
        dense_down,
        state,
        w_query,
        w_key,
        w_value,
        w_out,
        exp_gate[0].T,
        exp_up[0].T,
        exp_down[0],
    )
    return pl.pallas_call(
        finish,
        out_shape=(
            jax.ShapeDtypeStruct(tokens.shape, tokens.dtype),
            jax.ShapeDtypeStruct(state.shape, state.dtype),
        ),
        in_specs=[hbm] * 4,
        out_specs=(hbm, hbm),
        scratch_shapes=[
            buf(16, 1024, dtype=F32),
            buf(16, 256, dtype=F32),
            buf(16, 256, dtype=F32),
            buf(16, 1024),
            buf(16, 2, 128, 128, dtype=F32),
            pltpu.SemaphoreType.DMA((3,)),
            pltpu.SemaphoreType.DMA((8,)),
            pltpu.SemaphoreType.DMA((9,)),
        ],
        compiler_params=pltpu.CompilerParams(vmem_limit_bytes=67043328),
        name="finish",
    )(summed, key, value, state)


def solution(mesh):
    finer = Mesh(mesh.devices.reshape(8, 4, 4, mesh.shape["tp"]), (*EP, "tp"))
    in_specs = (
        P(EP, "tp"),
        P(EP, "tp", None, None),
        P(),
        P(None, "tp"),
        P(None, "tp"),
        P(None, "tp"),
        P("tp", None),
        P("tp"),
        P("tp"),
        P("tp", EP),
        P("tp", EP),
        P(EP, "tp"),
        P(EP, None, "tp"),
        P(EP, None, "tp"),
        P(EP, "tp", None),
        P(EP, None),
        P(EP, None),
    )
    out_specs = (P(EP, "tp"), P(EP, "tp", None, None))
    return jax.shard_map(body, mesh=finer, in_specs=in_specs, out_specs=out_specs, check_vma=False)
```

time: 93.5 us -> 65.1 us (0.70)
  local copies, waits for them, and re-layouts: 18.2 us -> 0 us
  Pallas kernels: 73.9 us -> 64.4 us
    unnamed x32 -> x0, local copies, waits for them, and re-layouts: 17.5 us -> none
    pallas_call x1 -> x2, Pallas kernels: 73.9 us -> 64.4 us  [the longest x1 60.8 us: body(): pl.pallas_call(kernel, out_shape=(jax.ShapeDtypeStruct(tokens.shape, F32)...]
where the time goes in v2:
time: 65.1 us; the launch traced here: 65 us
  Pallas kernels  64.4 us (99%)
    pallas_call x1, Pallas kernels, body(): pl.pallas_call(kernel, out_shape=(jax.ShapeDtypeStruct(tokens.shape, F32)...  60.8 us
    pallas_call x1, Pallas kernels, body(): pl.pallas_call(finish, out_shape=(jax.ShapeDtypeStruct(tokens.shape, toke...  3.51 us

profile of v2, /device:TPU:1, one launch (start us, length us, event | category | flops | bytes accessed | tf_op | source)
XLA Modules:
  0.0 65.0 jit_solution(16022141594540944421)
XLA Ops:
  0.6 60.8 %layer.1 = (f32[16,1024]{1,0:T(8,128)}, f32[16,256]{1,0:T(8,128)}, f32[16,256]{1,0:T(8,128)}) custom-call(bf16[16,1024]{1,0:T(8,128)(2,1)} %tokens_h.1, f32[1,2048]{1,0:T(1,128)} %bitcast.19, f32[1,1024]{1,0:T(1,128)} %bitcast.20, bf16[8,128]{1,0:T(8,128)(2,1)} %bitcast.21, s32[2,16]{1,0:T(2,128)} %bitcast.22, bf16[2,16]{1,0:T(2,128)(2,1)} %bitcast.23, ...), custom_call_target="tpu_custom_call" | custom-call | tf_op jit(solution)/shard_map/layer/pallas_call | solution.py:580
  61.5 3.5 %finish.1 = (bf16[16,1024]{1,0:T(8,128)(2,1)}, f32[16,2,128,128]{3,2,1,0:T(8,128)}) custom-call(f32[16,1024]{1,0:T(8,128)} %get-tuple-element.5.summed_h, f32[16,256]{1,0:T(8,128)} %get-tuple-element.6.key_h, f32[16,256]{1,0:T(8,128)} %get-tuple-element.7.value_h, f32[16,2,128,128]{3,2,1,0:T(8,128)} %state_h.1), custom_call_target="tpu_custom_call" | custom-call | tf_op jit(solution)/shard_map/finish/pallas_call | solution.py:648

commit v3 on v2

--- a/solution.py
+++ b/solution.py
@@ -39,8 +39,11 @@
     return v / (1.0 + jnp.exp(-v))
 
 
-def pack_matrix(row, col):
-    return jnp.where((row < 4 * CAP) & (col == row // CAP * SLOT + row % CAP), 1.0, 0.0).astype(BF16)
+def pack_matrix(row, col, half):
+    main = row < 32
+    slot = jnp.where(main, row % 16, 16 + row % 4)
+    part = jnp.where(main, row // 16, (row - 32) // 4)
+    return jnp.where((part == half) & (col == slot // CAP * SLOT + slot % CAP), 1.0, 0.0).astype(BF16)
 
 
 def kernel(
@@ -62,8 +65,7 @@
     eup,
     edown,
     mixed,
-    key_out,
-    value_out,
+    st,
     tokens,
     norm_mix,
     norm_ffn,
@@ -77,7 +79,6 @@
     wk,
     wv,
     wo,
-    st,
     read,
     tok_p,
     nf_p,
@@ -88,6 +89,7 @@
     disp,
     zrecv,
     xs,
+    sc,
     outs,
     opp_q,
     fin_q,
@@ -194,18 +196,12 @@
     pair = [started(tokens, tok_p, partner), started(norm_ffn, nf_p, partner)]
 
     def wd_slot(n):
-        return wd.at[:, pl.ds(c, 1), pl.ds(24 * n, 24), :]
+        return wd.at[:, pl.ds(c, 1), pl.ds(24 * (n - (n > 4)), 24), :]
 
     ring, cross = {}, {}
 
     def forward(source, target):
-        ring[target] = started(wd_slot(source), wd_slot(target), along_z(1 if target < 5 else -1))
-
-    def last(source, start, count, by):
-        def part(n):
-            return wd.at[pl.ds(start, count), pl.ds(c, 1), pl.ds(24 * n, 24), :]
-
-        ring[4, by] = started(part(source), part(4), along_z(by))
+        ring[target] = started(wd_slot(source), wd_slot(target), along_z(1 if target < 4 else -1))
 
     def across(n):
         cross[n] = started(wd_slot(n), wd_slot(n), partner)
@@ -226,8 +222,6 @@
     query = dot(normed, wq[...]).astype(BF16).astype(F32)
     key = dot(normed, wk[...]).astype(BF16).astype(F32) * 128 ** (-0.5)
     value = dot(normed, wv[...]).astype(BF16).astype(F32)
-    key_out[...] = key
-    value_out[...] = value
     blank = jnp.zeros((112, 256), F32)
     query_t = jnp.concatenate([query, blank], axis=0).T
     key_t = jnp.concatenate([key, blank], axis=0).T
@@ -239,6 +233,7 @@
             q_col = query_t[h * 128 : (h + 1) * 128, s : s + 1]
             v_row = value[s : s + 1, h * 128 : (h + 1) * 128]
             new = decay * st[s, h] + k_col * v_row
+            st[s, h] = new
             read[s : s + 1, h * 128 : (h + 1) * 128] = jnp.sum(q_col * new, axis=0, keepdims=True)
     heads = []
     for h in range(2):
@@ -261,9 +256,11 @@
     chosen = jnp.where(place == (block % SLOT).astype(F32), member, 0.0)
     weights = route_w[...].astype(F32)
     slot_w = jnp.sum(chosen * (hit0 * weights[0:1, :] + hit1 * weights[1:2, :]), axis=1, keepdims=True)
-    slot_first = jnp.sum(chosen * hit0, axis=1, keepdims=True)
-    lane = iota((64, 128), 1)
-    extra = jnp.where(lane == 0, slot_w, jnp.where(lane == 1, slot_first, 0.0))
+    other = jnp.where(hit0 > 0.0, routes[1:2, :], routes[0:1, :])
+    absent = lax.rem(expert - other + 12, 8)
+    absent = jnp.where(absent > 4, absent - 1, absent).astype(F32)
+    slot_absent = jnp.sum(chosen * absent, axis=1, keepdims=True)
+    extra = jnp.where(iota((64, 128), 1) % 2 == 0, slot_w, slot_absent)
     extra = jnp.where(first, extra[0:32, :], extra[32:64, :]).astype(BF16)
     mine = jnp.where(first, chosen[0:32, :], chosen[32:64, :]).astype(BF16)
 
@@ -280,16 +277,17 @@
     for j in range(4):
         part = pl.ds(SLOT * j, SLOT)
         moved.append(remote(disp.at[part], zrecv.at[part], along_z(-(4 * c + j))))
-    for j in (3, 2, 1):
-        moved[j].start()
 
     @pl.when(first)
     def _():
+        for j in (3, 2, 1):
+            moved[j].start()
         zrecv[0:SLOT, :] = disp[0:SLOT, :]
 
     @pl.when(jnp.logical_not(first))
     def _():
-        moved[0].start()
+        for j in range(4):
+            moved[j].start()
 
     ring[1].wait_recv()
     forward(1, 2)
@@ -305,111 +303,153 @@
     def _():
         moved[0].wait_recv()
 
-    def cell(ref, rq, rp, start=0, count=24):
-        return ref.at[pl.ds(24 * (4 * AT[rq] + rp) + start, count)]
+    def cell(ref, rq, rp):
+        return ref.at[4 * AT[rq] + rp]
 
     def cell_rows(ref, rq, rp):
-        base = 24 * (4 * AT[rq] + rp)
-        return ref[base : base + 24, :].astype(F32)
+        return ref[4 * AT[rq] + rp].astype(F32)
 
     def set_rows(ref, rq, rp, rows):
-        base = 24 * (4 * AT[rq] + rp)
-        ref[base : base + 24, :] = rows.astype(BF16)
-
-    set_rows(xs, 0, 0, dot(pack_matrix(iota((24, 32), 0), iota((24, 32), 1)), zrecv[...]))
+        ref[4 * AT[rq] + rp] = rows.astype(BF16)
+
+    row, col = iota((40, 32), 0), iota((40, 32), 1)
+    packed = dot(pack_matrix(row, col, 0), zrecv[:, 0:1024]) + dot(pack_matrix(row, col, 1), zrecv[:, 1024:2048])
+    set_rows(xs, 0, 0, packed)
+    lane8, row8, col8 = iota((8, 128), 1), iota((8, 32), 0), iota((8, 32), 1)
+
+    def scalars(slot):
+        pick = jnp.where(col8 == slot // CAP * SLOT + slot % CAP, 1.0, 0.0).astype(BF16)
+        return dot(pick, zrecv[:, 2048:2176])
+
+    packed_sc = jnp.where(
+        lane8 < 2, scalars(row8), jnp.where(lane8 < 4, scalars(row8 + 8), scalars(16 + row8 % 4))
+    )
+    set_rows(sc, 0, 0, packed_sc)
 
     got = {}
 
+    def spread(from_q, from_p, to_q, to_p, device):
+        got[to_q, to_p] = [
+            started(cell(ref, from_q, from_p), cell(ref, to_q, to_p), device) for ref in (sc, xs)
+        ]
+
+    def arrived(rq, rp):
+        for copy in got[rq, rp]:
+            copy.wait_recv()
+
     def send_q(rp):
-        got[1, rp] = started(cell(xs, 0, rp), cell(xs, 1, rp), along_q(1))
-        got[3, rp] = started(cell(xs, 0, rp), cell(xs, 3, rp), along_q(-1))
+        spread(0, rp, 1, rp, along_q(1))
+        spread(0, rp, 3, rp, along_q(-1))
 
     def pass_on(rp):
         by = PASS[rp]
-        near = 2 - by
-        got[near, rp].wait_recv()
-        got[2, rp] = started(cell(xs, near, rp), cell(xs, 2, rp), along_q(by))
-
-    got[0, 1] = started(cell(xs, 0, 0), cell(xs, 0, 1), along_p(1))
-    got[0, 3] = started(cell(xs, 0, 0), cell(xs, 0, 3), along_p(-1))
-    got[0, 2] = started(cell(xs, 0, 0), cell(xs, 0, 2), along_p(2))
+        arrived(2 - by, rp)
+        spread(2 - by, rp, 2, rp, along_q(by))
+
+    spread(0, 0, 0, 1, along_p(1))
+    spread(0, 0, 0, 3, along_p(-1))
+    spread(0, 0, 0, 2, along_p(2))
     send_q(0)
-    got[0, 1].wait_recv()
+    arrived(0, 1)
     send_q(1)
-    got[0, 3].wait_recv()
-    send_q(3)
-    pass_on(0)
     ring[2].wait_recv()
     forward(2, 3)
     ring[6].wait_recv()
     forward(6, 5)
     across(2)
     across(6)
-    got[0, 2].wait_recv()
+    arrived(0, 3)
+    send_q(3)
+    pass_on(0)
+    arrived(0, 2)
     send_q(2)
-    got[2, 2] = started(cell(xs, 0, 2), cell(xs, 2, 2), along_q(2))
+    spread(0, 2, 2, 2, along_q(2))
     pass_on(1)
     pass_on(3)
-    ring[3].wait_recv()
-    last(3, 0, 2, 1)
-    across(3)
-    ring[5].wait_recv()
-    last(5, 2, 1, -1)
-    across(5)
+    for n in (3, 5):
+        ring[n].wait_recv()
+        across(n)
     for rp in range(4):
         for rq in (1, 3):
             if rp == 2 or PASS[rp] != 2 - rq:
-                got[rq, rp].wait_recv()
+                arrived(rq, rp)
 
     for n in (14, 15, 16):
         loads[n].wait()
     for copy in swap:
         copy.wait_recv()
 
-    def hidden_rows(start, count):
-        rows = xs[start : start + count, 0:2048]
-        scale = xs[start : start + count, 2048:2049].astype(F32)
-        return (silu(dot_nt(rows, we[0])) * dot_nt(rows, we[1]) * scale).astype(BF16)
-
-    hidden_near = hidden_rows(96, 288)
+    def operands(start, count):
+        rest = xs[start : start + count, 32:40, :].reshape(8 * count, 1024)
+        main = [xs[start : start + count, 16 * h : 16 * h + 16, :].reshape(16 * count, 1024) for h in range(2)]
+        return [jnp.concatenate([part, rest], axis=0) for part in main]
+
+    def product(pair, w_lo, w_hi):
+        lo, hi = dot_nt(pair[0], w_lo), dot_nt(pair[1], w_hi)
+        main = lo.shape[0] // 3 * 2
+        rest_lo, rest_hi = lo[main:, :], hi[main:, :]
+        count = rest_lo.shape[0]
+        top = iota((count, 1), 0) % 8 < 4
+        rest = jnp.where(top, rest_lo, pltpu.roll(rest_lo, 4, 0)) + jnp.where(
+            top, pltpu.roll(rest_hi, count - 4, 0), rest_hi
+        )
+        return jnp.concatenate([lo[0:main, :] + hi[0:main, :], rest], axis=0)
+
+    def column(start, count, lane):
+        tiles = sc[start : start + count].astype(F32)
+        main = jnp.concatenate([tiles[:, :, lane : lane + 1], tiles[:, :, lane + 2 : lane + 3]], axis=1)
+        rest = tiles[:, :, lane + 4 : lane + 5]
+        return jnp.concatenate([main.reshape(16 * count, 1), rest.reshape(8 * count, 1)], axis=0)
+
+    def expert_rows(pair, start, count):
+        gate, up = (product(pair, we[t, :, 0:1024], we[t, :, 1024:2048]) for t in range(2))
+        return (silu(gate) * up * column(start, count, 0)).astype(BF16)
+
+    def dense_rows(pair, start, count):
+        gate, up = (product(pair, wd[t, 0], wd[t, 1]) for t in range(2))
+        share = jnp.where(iota(gate.shape, 1) // 24 == column(start, count, 1).astype(jnp.int32), 1.0, 0.5)
+        return (silu(gate) * up * (share / (1.0 + jnp.exp(-gate[:, 22:23])))).astype(BF16)
+
+    near = operands(4, 12)
+    near_e = expert_rows(near, 4, 12)
+    for copy in cross.values():
+        copy.wait_recv()
+    near_d = dense_rows(near, 4, 12)
     for rp in range(4):
-        got[2, rp].wait_recv()
-    hidden_far = hidden_rows(0, 96)
-
-    ring[4, 1].wait_recv()
-    ring[4, -1].wait_recv()
-    across(4)
-    for n in range(8):
-        cross[n].wait_recv()
-
-    def dense_pre(t):
-        return dot_nt(xs[:, 0:1024], wd[t, 0]) + dot_nt(xs[:, 1024:2048], wd[t, 1])
-
-    pre = dense_pre(0)
-    dense_scale = xs[:, 2049:2050].astype(F32) / (1.0 + jnp.exp(-pre[:, 22:23]))
-    hidden_d = (silu(pre) * dense_pre(1) * dense_scale).astype(BF16)
-
-    def down(hidden_e, start, count):
-        take = slice(start, start + count)
-        for n in range(4):
-            outs[take, 512 * n : 512 * (n + 1)] = (
-                dot(hidden_e, we[2, :, 512 * n : 512 * (n + 1)])
-                + dot(hidden_d[take, :], wd[2, n // 2, :, 512 * (n % 2) : 512 * (n % 2 + 1)])
-            ).astype(BF16)
+        arrived(2, rp)
+    far = operands(0, 4)
+    far_e = expert_rows(far, 0, 4)
+    far_d = dense_rows(far, 0, 4)
+
+    def down(hidden_e, hidden_d, start, count):
+        main = 16 * count
+        top = iota((8 * count, 1), 0) % 8 < 4
+        for n in range(2):
+            cols = slice(512 * n, 512 * n + 512)
+            part = [
+                dot(hidden_e, we[2, :, 1024 * h + 512 * n : 1024 * h + 512 * n + 512]) + dot(hidden_d, wd[2, h, :, cols])
+                for h in range(2)
+            ]
+            for h in range(2):
+                outs[start : start + count, 16 * h : 16 * h + 16, cols] = (
+                    part[h][0:main, :].astype(BF16).reshape(count, 16, 512)
+                )
+            rest = jnp.where(top, part[0][main:, :], part[1][main:, :])
+            outs[start : start + count, 32:40, cols] = rest.reshape(count, 8, 512).astype(BF16)
 
     back = {}
 
     def at_rp(ref, rp):
-        return ref.at[pl.ds(24 * rp, 24)]
+        return ref.at[rp]
 
     def rp_rows(ref, rp):
-        return ref[24 * rp : 24 * rp + 24, :].astype(F32)
-
-    down(hidden_far, 0, 96)
+        return ref[rp].astype(F32)
+
+    down(far_e, far_d, 0, 4)
     direct = started(cell(outs, 2, 2), at_rp(opp_q, 2), along_q(2))
     for rp in (1, 3, 0):
         back[2, rp] = started(cell(outs, 2, rp), at_rp(opp_q, rp), along_q(-PASS[rp]))
-    down(hidden_near, 96, 288)
+    down(near_e, near_d, 4, 12)
 
     def send_back(rq, rp):
         back[rq, rp] = started(cell(outs, rq, rp), at_rp(fin_q.at[rq // 2], rp), along_q(-1 if rq == 1 else 1))
@@ -431,9 +471,8 @@
         total[rp] = cell_rows(outs, 0, rp) + rp_rows(fin_q.at[0], rp) + rp_rows(fin_q.at[1], rp)
 
     def send_p(n, rp, by):
-        rows = pl.ds(24 * n, 24)
-        tsend[24 * n : 24 * n + 24, :] = total[rp].astype(BF16)
-        back["p", n] = started(tsend.at[rows], fin_p.at[rows], along_p(by))
+        tsend[n] = total[rp].astype(BF16)
+        back["p", n] = started(tsend.at[n], fin_p.at[n], along_p(by))
 
     sum_q(2)
     direct.wait_recv()
@@ -448,9 +487,8 @@
         back["p", n].wait_recv()
     summed = (total[0] + rp_rows(fin_p, 0) + rp_rows(fin_p, 1) + rp_rows(fin_p, 2)).astype(BF16)
 
-    opened = dot(pack_matrix(iota((32, 24), 1), iota((32, 24), 0)), summed)
     for h in range(2):
-        rbuf[h] = opened[:, 1024 * h : 1024 * (h + 1)].astype(BF16)
+        rbuf[h] = dot(pack_matrix(iota((32, 40), 1), iota((32, 40), 0), h), summed).astype(BF16)
 
     def ret_copy(j, h, device):
         d = 4 * c + j
@@ -467,18 +505,18 @@
         return {**along_z(4 * c + j), "tp": h}
 
     def ret_each(act):
-        for j in (3, 2, 1):
-            for h in range(2):
-                act(ret_copy(j, h, ret_device(j, h)))
-
         @pl.when(first)
         def _():
+            for j in (3, 2, 1):
+                for h in range(2):
+                    act(ret_copy(j, h, ret_device(j, h)))
             act(ret_copy(0, 1, {"tp": 1}))
 
         @pl.when(jnp.logical_not(first))
         def _():
-            for h in range(2):
-                act(ret_copy(0, h, ret_device(0, h)))
+            for j in range(4):
+                for h in range(2):
+                    act(ret_copy(j, h, ret_device(j, h)))
 
     ret_each(lambda copy: copy.start())
 
@@ -504,7 +542,7 @@
     def _():
         ret_wait(0)
 
-    mixed[...] = after_own + dot_tn(chosen.astype(BF16), ret[...])
+    mixed[...] = (after_own + dot_tn(chosen.astype(BF16), ret[...])).astype(BF16)
 
     for copy in sent:
         copy.wait_send()
@@ -517,39 +555,6 @@
 
     ret_each(lambda copy: copy.wait_send())
     assert used[0] <= COPIES
-
-
-def finish(summed_h, key_h, value_h, state_h, mixed_h, new_h, summed, key, value, mixed, st, sem, in_sem, out_sem):
-    small = [
-        pltpu.make_async_copy(src, dst, sem.at[n])
-        for n, (src, dst) in enumerate(((key_h, key), (value_h, value), (summed_h, summed)))
-    ]
-    for copy in small:
-        copy.start()
-    pieces = []
-    for n in range(8):
-        part = pl.ds(2 * n, 2)
-        pieces.append(pltpu.make_async_copy(state_h.at[part], st.at[part], in_sem.at[n]))
-        pieces[n].start()
-    for copy in small:
-        copy.wait()
-    mixed[...] = summed[...].astype(BF16)
-    stores = [pltpu.make_async_copy(mixed, mixed_h, out_sem.at[8])]
-    stores[0].start()
-    key_t = jnp.concatenate([key[...], jnp.zeros((112, 256), F32)], axis=0).T
-    first = lax.axis_index("tp") == 0
-    decay = [jnp.where(first, 1.0 - 2.0 ** (-3.0 - 2.0 * h), 1.0 - 2.0 ** (-7.0 - 2.0 * h)) for h in range(2)]
-    for n in range(8):
-        pieces[n].wait()
-        for s in (2 * n, 2 * n + 1):
-            for h in range(2):
-                span = slice(128 * h, 128 * h + 128)
-                st[s, h] = decay[h] * st[s, h] + key_t[span, s : s + 1] * value[s : s + 1, span]
-        part = pl.ds(2 * n, 2)
-        stores.append(pltpu.make_async_copy(st.at[part], new_h.at[part], out_sem.at[n]))
-        stores[-1].start()
-    for copy in stores:
-        copy.wait()
 
 
 def body(
@@ -577,15 +582,14 @@
     def buf(*shape, dtype=BF16):
         return pltpu.VMEM(shape, dtype)
 
-    summed, key, value = pl.pallas_call(
+    return pl.pallas_call(
         kernel,
         out_shape=(
-            jax.ShapeDtypeStruct(tokens.shape, F32),
-            jax.ShapeDtypeStruct((16, 256), F32),
-            jax.ShapeDtypeStruct((16, 256), F32),
+            pltpu.VMEM(tokens.shape, tokens.dtype),
+            pltpu.VMEM(state.shape, state.dtype),
         ),
         in_specs=[hbm] * 17,
-        out_specs=(vmem, vmem, vmem),
+        out_specs=(vmem, vmem),
         scratch_shapes=[
             buf(16, 1024),
             buf(1, 2048, dtype=F32),
@@ -600,22 +604,22 @@
             buf(2048, 256),
             buf(2048, 256),
             buf(256, 2048),
-            buf(16, 2, 128, 128, dtype=F32),
             buf(16, 256, dtype=F32),
             buf(16, 1024),
             buf(1, 1024, dtype=F32),
             buf(16, 2048),
             buf(16, 2048),
             buf(3, 176, 2048),
-            buf(3, 2, 192, 1024),
+            buf(3, 2, 168, 1024),
             buf(32, 2176),
             buf(32, 2176),
-            buf(384, 2176),
-            buf(384, 2048),
-            buf(96, 2048),
-            buf(2, 96, 2048),
-            buf(72, 2048),
-            buf(72, 2048),
+            buf(16, 40, 1024),
+            buf(16, 8, 128),
+            buf(16, 40, 1024),
+            buf(4, 40, 1024),
+            buf(2, 4, 40, 1024),
+            buf(3, 40, 1024),
+            buf(3, 40, 1024),
             buf(2, 32, 1024),
             buf(64, 1024),
             pltpu.SemaphoreType.DMA((17,)),
@@ -624,48 +628,32 @@
             pltpu.SemaphoreType.DMA((8,)),
             pltpu.SemaphoreType.DMA((8,)),
         ],
-        compiler_params=pltpu.CompilerParams(collective_id=0, has_side_effects=True, vmem_limit_bytes=67043328),
+        compiler_params=pltpu.CompilerParams(collective_id=0, has_side_effects=True, vmem_limit_bytes=56 * 1024 * 1024),
         name="layer",
     )(
-        tokens,
-        norm_mix.reshape(1, -1),
-        norm_ffn.reshape(1, -1),
-        gate_vector.reshape(8, 128),
-        routes.T,
-        route_w.T,
-        dense_gate.T,
-        dense_up.T,
-        dense_down,
-        state,
-        w_query,
-        w_key,
-        w_value,
-        w_out,
-        exp_gate[0].T,
-        exp_up[0].T,
-        exp_down[0],
+        *(
+            pltpu.with_memory_space_constraint(operand, pltpu.HBM)
+            for operand in (
+                tokens,
+                norm_mix.reshape(1, -1),
+                norm_ffn.reshape(1, -1),
+                gate_vector.reshape(8, 128),
+                routes.T,
+                route_w.T,
+                dense_gate.T,
+                dense_up.T,
+                dense_down,
+                state,
+                w_query,
+                w_key,
+                w_value,
+                w_out,
+                exp_gate[0].T,
+                exp_up[0].T,
+                exp_down[0],
+            )
+        )
     )
-    return pl.pallas_call(
-        finish,
-        out_shape=(
-            jax.ShapeDtypeStruct(tokens.shape, tokens.dtype),
-            jax.ShapeDtypeStruct(state.shape, state.dtype),
-        ),
-        in_specs=[hbm] * 4,
-        out_specs=(hbm, hbm),
-        scratch_shapes=[
-            buf(16, 1024, dtype=F32),
-            buf(16, 256, dtype=F32),
-            buf(16, 256, dtype=F32),
-            buf(16, 1024),
-            buf(16, 2, 128, 128, dtype=F32),
-            pltpu.SemaphoreType.DMA((3,)),
-            pltpu.SemaphoreType.DMA((8,)),
-            pltpu.SemaphoreType.DMA((9,)),
-        ],
-        compiler_params=pltpu.CompilerParams(vmem_limit_bytes=67043328),
-        name="finish",
-    )(summed, key, value, state)
 
 
 def solution(mesh):

time: 65.1 us -> 60.7 us (0.932)
  Pallas kernels: 64.4 us -> 58 us
  local copies, waits for them, and re-layouts: 0 us -> 1.94 us
    pallas_call x2 -> x1, Pallas kernels: 64.4 us -> 58 us  [body(): pl.pallas_call(kernel, out_shape=(pltpu.VMEM(tokens.shape, tokens.dtype),...]
    unnamed x0 -> x2, local copies, waits for them, and re-layouts: none -> 1.94 us
where the time goes in v3:
time: 60.7 us; the launch traced here: 60.6 us
  Pallas kernels  58 us (96%)
  local copies, waits for them, and re-layouts  1.94 us (3%)
  between operations  0.65 us (1%)
    pallas_call x1, Pallas kernels, body(): pl.pallas_call(kernel, out_shape=(pltpu.VMEM(tokens.shape, tokens.dtype),...  58 us
    unnamed x2, local copies, waits for them, and re-layouts  1.94 us

profile of v3, /device:TPU:1, one launch (start us, length us, event | category | flops | bytes accessed | tf_op | source)
XLA Modules:
  0.0 60.6 jit_solution(10438361204082437907)
XLA Ops:
  0.6 58.0 %layer.1 = (bf16[16,1024]{1,0:T(8,128)(2,1)S(1)}, f32[16,2,128,128]{3,2,1,0:T(8,128)S(1)}) custom-call(bf16[16,1024]{1,0:T(8,128)(2,1)} %tokens_h.1, f32[1,2048]{1,0:T(1,128)} %bitcast.19, f32[1,1024]{1,0:T(1,128)} %bitcast.20, bf16[8,128]{1,0:T(8,128)(2,1)} %bitcast.21, s32[2,16]{1,0:T(2,128)} %bitcast.22, bf16[2,16]{1,0:T(2,128)(2,1)} %bitcast.23, ...), custom_call_target="tpu_custom_call" | custom-call | tf_op jit(solution)/shard_map/layer/pallas_call | solution.py:585
  58.7 0.6 %copy.21 = bf16[16,1024]{1,0:T(8,128)(2,1)} copy(bf16[16,1024]{1,0:T(8,128)(2,1)S(1)} %get-tuple-element.2) | data formatting | bytes 65536
  59.3 1.3 %copy.22 = f32[16,2,128,128]{3,2,1,0:T(8,128)} copy(f32[16,2,128,128]{3,2,1,0:T(8,128)S(1)} %get-tuple-element.3) | data formatting | bytes 4194304

commit v4 on v3

--- a/solution.py
+++ b/solution.py
@@ -14,7 +14,7 @@
 F32 = jnp.float32
 BF16 = jnp.bfloat16
 epsilon = 1e-06
-COPIES = 80
+COPIES = 112
 AT = {2: 0, 1: 1, 3: 2, 0: 3}
 PASS = {0: -1, 1: 1, 3: -1}
 
@@ -102,6 +102,7 @@
     recv_sem,
     ret_send,
     ret_recv,
+    known,
 ):
     z, y, x, c = (lax.axis_index(a) for a in (Z, Y, X, "tp"))
     first = c == 0
@@ -175,11 +176,8 @@
 
     barrier = pltpu.get_barrier_semaphore()
     peers = [partner]
-    for by in range(1, 8):
-        for core in (c, 1 - c):
-            peers.append({**along_z(by), "tp": core})
-    for by in (1, -1, 2):
-        peers += [along_p(by), along_q(by)]
+    for by in (1, -1):
+        peers += [along_z(by), along_p(by), along_q(by)]
     for peer in peers:
         pl.semaphore_signal(barrier, inc=1, device_id=peer, device_id_type=MESH)
 
@@ -192,6 +190,23 @@
         wd[t, pl.ds(c, 1), pl.ds(0, 24), :] = block.astype(BF16)[None]
 
     pl.semaphore_wait(barrier, len(peers))
+
+    def tell(n, device):
+        pl.semaphore_signal(known.at[n], inc=1, device_id=device, device_id_type=MESH)
+
+    def hear(n):
+        pl.semaphore_wait(known.at[n], 1)
+
+    tell(0, along_z(1))
+    tell(3, along_z(-1))
+    tell(6, along_p(1))
+    tell(7, along_q(1))
+
+    def relay(n):
+        for start, by in ((0, 1), (3, -1)):
+            hear(start + n)
+            tell(start + n + 1, along_z(by))
+
 
     pair = [started(tokens, tok_p, partner), started(norm_ffn, nf_p, partner)]
 
@@ -225,19 +240,18 @@
     blank = jnp.zeros((112, 256), F32)
     query_t = jnp.concatenate([query, blank], axis=0).T
     key_t = jnp.concatenate([key, blank], axis=0).T
+    relay(0)
     loads[12].wait()
+    decay = [jnp.where(first, 1.0 - 2.0 ** (-3.0 - 2.0 * h), 1.0 - 2.0 ** (-7.0 - 2.0 * h)) for h in range(2)]
     for h in range(2):
-        decay = jnp.where(first, 1.0 - 2.0 ** (-3.0 - 2.0 * h), 1.0 - 2.0 ** (-7.0 - 2.0 * h))
+        span = slice(128 * h, 128 * h + 128)
         for s in range(16):
-            k_col = key_t[h * 128 : (h + 1) * 128, s : s + 1]
-            q_col = query_t[h * 128 : (h + 1) * 128, s : s + 1]
-            v_row = value[s : s + 1, h * 128 : (h + 1) * 128]
-            new = decay * st[s, h] + k_col * v_row
-            st[s, h] = new
-            read[s : s + 1, h * 128 : (h + 1) * 128] = jnp.sum(q_col * new, axis=0, keepdims=True)
+            read[s : s + 1, span] = jnp.sum(query_t[span, s : s + 1] * st[s, h], axis=0, keepdims=True)
     heads = []
     for h in range(2):
-        part = read[:, h * 128 : (h + 1) * 128]
+        span = slice(128 * h, 128 * h + 128)
+        met = jnp.sum(query[:, span] * key[:, span], axis=1, keepdims=True)
+        part = decay[h] * read[:, span] + met * value[:, span]
         centre = jnp.mean(part, axis=1, keepdims=True)
         spread = jnp.mean(jnp.square(part - centre), axis=1, keepdims=True)
         heads.append(((part - centre) * lax.rsqrt(spread + epsilon)).astype(BF16))
@@ -264,12 +278,15 @@
     extra = jnp.where(first, extra[0:32, :], extra[32:64, :]).astype(BF16)
     mine = jnp.where(first, chosen[0:32, :], chosen[32:64, :]).astype(BF16)
 
+    relay(1)
     mix_copy.wait_recv()
     after = (full + (mix_o[...].astype(F32) + mix_p[...].astype(F32))).astype(BF16).astype(F32)
     mean2 = jnp.sum(after * after, axis=1, keepdims=True) / 2048.0
     nf_lo, nf_hi = halves(norm_ffn[...], nf_p[...])
     normed2 = (after * lax.rsqrt(mean2 + epsilon) * jnp.concatenate([nf_lo, nf_hi], axis=1)).astype(BF16)
 
+    hear(2)
+    hear(5)
     rows = dot(mine, normed2)
     disp[:, 2048:2176] = extra
     disp[:, 0:2048] = rows.astype(BF16)
@@ -289,13 +306,17 @@
         for j in range(4):
             moved[j].start()
 
+    for h in range(2):
+        span = slice(128 * h, 128 * h + 128)
+        for s in range(16):
+            st[s, h] = decay[h] * st[s, h] + key_t[span, s : s + 1] * value[s : s + 1, span]
+
     ring[1].wait_recv()
     forward(1, 2)
     ring[7].wait_recv()
     forward(7, 6)
     across(1)
     across(7)
-
     for j in (1, 2, 3):
         moved[j].wait_recv()
 
@@ -328,52 +349,51 @@
 
     got = {}
 
-    def spread(from_q, from_p, to_q, to_p, device):
-        got[to_q, to_p] = [
-            started(cell(ref, from_q, from_p), cell(ref, to_q, to_p), device) for ref in (sc, xs)
-        ]
-
-    def arrived(rq, rp):
-        for copy in got[rq, rp]:
-            copy.wait_recv()
-
-    def send_q(rp):
-        spread(0, rp, 1, rp, along_q(1))
-        spread(0, rp, 3, rp, along_q(-1))
-
-    def pass_on(rp):
+    def chunk(ref, rq, rp, n):
+        return ref.at[4 * AT[rq] + rp, :, pl.ds(512 * n, 512)]
+
+    def spread(from_q, from_p, to_q, to_p, n, device):
+        got[to_q, to_p, n] = started(chunk(xs, from_q, from_p, n), chunk(xs, to_q, to_p, n), device)
+        if n == 0:
+            got[to_q, to_p, 2] = started(cell(sc, from_q, from_p), cell(sc, to_q, to_p), device)
+
+    def arrived(rq, rp, n):
+        got[rq, rp, n].wait_recv()
+        if n == 0:
+            got[rq, rp, 2].wait_recv()
+
+    def send_q(rp, n):
+        spread(0, rp, 1, rp, n, along_q(1))
+        spread(0, rp, 3, rp, n, along_q(-1))
+
+    def pass_on(rp, n):
         by = PASS[rp]
-        arrived(2 - by, rp)
-        spread(2 - by, rp, 2, rp, along_q(by))
-
-    spread(0, 0, 0, 1, along_p(1))
-    spread(0, 0, 0, 3, along_p(-1))
-    spread(0, 0, 0, 2, along_p(2))
-    send_q(0)
-    arrived(0, 1)
-    send_q(1)
+        arrived(2 - by, rp, n)
+        spread(2 - by, rp, 2, rp, n, along_q(by))
+
+    hear(6)
+    hear(7)
+    for n in range(2):
+        spread(0, 0, 0, 1, n, along_p(1))
+        spread(0, 0, 0, 3, n, along_p(-1))
+        send_q(0, n)
+        spread(0, 0, 0, 2, n, along_p(2))
+    for n in range(2):
+        arrived(0, 1, n)
+        send_q(1, n)
+        arrived(0, 3, n)
+        send_q(3, n)
+        pass_on(0, n)
+    for n in range(2):
+        arrived(0, 2, n)
+        send_q(2, n)
+        spread(0, 2, 2, 2, n, along_q(2))
     ring[2].wait_recv()
     forward(2, 3)
     ring[6].wait_recv()
     forward(6, 5)
     across(2)
     across(6)
-    arrived(0, 3)
-    send_q(3)
-    pass_on(0)
-    arrived(0, 2)
-    send_q(2)
-    spread(0, 2, 2, 2, along_q(2))
-    pass_on(1)
-    pass_on(3)
-    for n in (3, 5):
-        ring[n].wait_recv()
-        across(n)
-    for rp in range(4):
-        for rq in (1, 3):
-            if rp == 2 or PASS[rp] != 2 - rq:
-                arrived(rq, rp)
-
     for n in (14, 15, 16):
         loads[n].wait()
     for copy in swap:
@@ -410,18 +430,35 @@
         share = jnp.where(iota(gate.shape, 1) // 24 == column(start, count, 1).astype(jnp.int32), 1.0, 0.5)
         return (silu(gate) * up * (share / (1.0 + jnp.exp(-gate[:, 22:23])))).astype(BF16)
 
-    near = operands(4, 12)
-    near_e = expert_rows(near, 4, 12)
+    own = operands(12, 4)
+    own_e = expert_rows(own, 12, 4)
+    for n in range(2):
+        pass_on(1, n)
+        pass_on(3, n)
+    for n in (3, 5):
+        ring[n].wait_recv()
+        across(n)
     for copy in cross.values():
         copy.wait_recv()
-    near_d = dense_rows(near, 4, 12)
-    for rp in range(4):
-        arrived(2, rp)
-    far = operands(0, 4)
-    far_e = expert_rows(far, 0, 4)
-    far_d = dense_rows(far, 0, 4)
-
-    def down(hidden_e, hidden_d, start, count):
+    own_d = dense_rows(own, 12, 4)
+    for n in range(2):
+        for rp in range(4):
+            for rq in (1, 3):
+                if rp == 2 or PASS[rp] != 2 - rq:
+                    arrived(rq, rp, n)
+    for n in range(2):
+        for rp in range(4):
+            arrived(2, rp, n)
+    rest = operands(0, 12)
+    rest_e = expert_rows(rest, 0, 12)
+    rest_d = dense_rows(rest, 0, 12)
+
+    def blocks(rows, start, count):
+        return jnp.concatenate(
+            [rows[16 * start : 16 * (start + count), :], rows[192 + 8 * start : 192 + 8 * (start + count), :]], axis=0
+        )
+
+    def down(hidden_e, hidden_d, start, count, then):
         main = 16 * count
         top = iota((8 * count, 1), 0) % 8 < 4
         for n in range(2):
@@ -436,56 +473,72 @@
                 )
             rest = jnp.where(top, part[0][main:, :], part[1][main:, :])
             outs[start : start + count, 32:40, cols] = rest.reshape(count, 8, 512).astype(BF16)
+            then(n)
 
     back = {}
 
-    def at_rp(ref, rp):
-        return ref.at[rp]
-
-    def rp_rows(ref, rp):
-        return ref[rp].astype(F32)
-
-    down(far_e, far_d, 0, 4)
-    direct = started(cell(outs, 2, 2), at_rp(opp_q, 2), along_q(2))
-    for rp in (1, 3, 0):
-        back[2, rp] = started(cell(outs, 2, rp), at_rp(opp_q, rp), along_q(-PASS[rp]))
-    down(near_e, near_d, 4, 12)
-
-    def send_back(rq, rp):
-        back[rq, rp] = started(cell(outs, rq, rp), at_rp(fin_q.at[rq // 2], rp), along_q(-1 if rq == 1 else 1))
-
-    for rq, rp in ((1, 2), (3, 2), (1, 1), (3, 1), (1, 3), (3, 3), (1, 0), (3, 0)):
-        if rp == 2 or PASS[rp] != 2 - rq:
-            send_back(rq, rp)
-    for rp in (1, 3, 0):
-        rq = 2 - PASS[rp]
-        back[2, rp].wait_recv()
-        set_rows(outs, rq, rp, cell_rows(outs, rq, rp) + rp_rows(opp_q, rp))
-        send_back(rq, rp)
+    def part(ref, rp, n):
+        return ref.at[rp, :, pl.ds(512 * n, 512)]
+
+    def part_rows(ref, rp, n):
+        return ref[rp, :, 512 * n : 512 * n + 512].astype(F32)
+
+    def send_far(n):
+        back["far", n] = started(chunk(outs, 2, 2, n), part(opp_q, 2, n), along_q(2))
+        for rp in (1, 3, 0):
+            back[2, rp, n] = started(chunk(outs, 2, rp, n), part(opp_q, rp, n), along_q(-PASS[rp]))
+
+    def send_back(rq, rp, n):
+        device = along_q(-1 if rq == 1 else 1)
+        back[rq, rp, n] = started(chunk(outs, rq, rp, n), part(fin_q.at[rq // 2], rp, n), device)
+
+    def send_near(n):
+        for rq, rp in ((1, 2), (3, 2), (1, 1), (3, 1), (1, 3), (3, 3), (1, 0), (3, 0)):
+            if rp == 2 or PASS[rp] != 2 - rq:
+                send_back(rq, rp, n)
+
+    down(blocks(rest_e, 0, 4), blocks(rest_d, 0, 4), 0, 4, send_far)
+    down(blocks(rest_e, 4, 8), blocks(rest_d, 4, 8), 4, 8, send_near)
+    down(own_e, own_d, 12, 4, lambda n: None)
+    for n in range(2):
+        for rp in (1, 3, 0):
+            rq = 2 - PASS[rp]
+            at = 4 * AT[rq] + rp
+            back[2, rp, n].wait_recv()
+            both = part_rows(outs, at, n) + part_rows(opp_q, rp, n)
+            outs[at, :, 512 * n : 512 * n + 512] = both.astype(BF16)
+            send_back(rq, rp, n)
 
     total = {}
 
-    def sum_q(rp):
+    def sum_q(rp, n):
         for rq in (1, 3):
-            back[rq, rp].wait_recv()
-        total[rp] = cell_rows(outs, 0, rp) + rp_rows(fin_q.at[0], rp) + rp_rows(fin_q.at[1], rp)
-
-    def send_p(n, rp, by):
-        tsend[n] = total[rp].astype(BF16)
-        back["p", n] = started(tsend.at[n], fin_p.at[n], along_p(by))
-
-    sum_q(2)
-    direct.wait_recv()
-    total[2] = total[2] + rp_rows(opp_q, 2)
-    send_p(0, 2, 2)
-    sum_q(1)
-    send_p(1, 1, -1)
-    sum_q(3)
-    send_p(2, 3, 1)
-    sum_q(0)
-    for n in range(3):
-        back["p", n].wait_recv()
-    summed = (total[0] + rp_rows(fin_p, 0) + rp_rows(fin_p, 1) + rp_rows(fin_p, 2)).astype(BF16)
+            back[rq, rp, n].wait_recv()
+        own_part = part_rows(outs, 4 * AT[0] + rp, n)
+        total[rp, n] = own_part + part_rows(fin_q.at[0], rp, n) + part_rows(fin_q.at[1], rp, n)
+
+    def send_p(slot, rp, n, by):
+        tsend[slot, :, 512 * n : 512 * n + 512] = total[rp, n].astype(BF16)
+        back["p", slot, n] = started(part(tsend, slot, n), part(fin_p, slot, n), along_p(by))
+
+    for n in range(2):
+        sum_q(2, n)
+        back["far", n].wait_recv()
+        total[2, n] = total[2, n] + part_rows(opp_q, 2, n)
+        send_p(0, 2, n, 2)
+    for n in range(2):
+        sum_q(1, n)
+        send_p(1, 1, n, -1)
+        sum_q(3, n)
+        send_p(2, 3, n, 1)
+    for n in range(2):
+        sum_q(0, n)
+    ends = []
+    for n in range(2):
+        for slot in range(3):
+            back["p", slot, n].wait_recv()
+        ends.append(total[0, n] + part_rows(fin_p, 0, n) + part_rows(fin_p, 1, n) + part_rows(fin_p, 2, n))
+    summed = jnp.concatenate(ends, axis=1).astype(BF16)
 
     for h in range(2):
         rbuf[h] = dot(pack_matrix(iota((32, 40), 1), iota((32, 40), 0), h), summed).astype(BF16)
@@ -627,6 +680,7 @@
             pltpu.SemaphoreType.DMA((COPIES,)),
             pltpu.SemaphoreType.DMA((8,)),
             pltpu.SemaphoreType.DMA((8,)),
+            pltpu.SemaphoreType.REGULAR((8,)),
         ],
         compiler_params=pltpu.CompilerParams(collective_id=0, has_side_effects=True, vmem_limit_bytes=56 * 1024 * 1024),
         name="layer",

time: 60.7 us -> 58.3 us (0.960)
  Pallas kernels: 58 us -> 55.6 us
    pallas_call x1, Pallas kernels: 58 us -> 55.6 us  [body(): pl.pallas_call(kernel, out_shape=(pltpu.VMEM(tokens.shape, tokens.dtype),...]
where the time goes in v4:
time: 58.3 us; the launch traced here: 58.2 us
  Pallas kernels  55.6 us (95%)
  local copies, waits for them, and re-layouts  1.94 us (3%)
  between operations  0.65 us (1%)
    pallas_call x1, Pallas kernels, body(): pl.pallas_call(kernel, out_shape=(pltpu.VMEM(tokens.shape, tokens.dtype),...  55.6 us
    unnamed x2, local copies, waits for them, and re-layouts  1.94 us

profile of v4, /device:TPU:1, one launch (start us, length us, event | category | flops | bytes accessed | tf_op | source)
XLA Modules:
  0.0 58.2 jit_solution(10422205244305496017)
XLA Ops:
  0.6 55.6 %layer.1 = (bf16[16,1024]{1,0:T(8,128)(2,1)S(1)}, f32[16,2,128,128]{3,2,1,0:T(8,128)S(1)}) custom-call(bf16[16,1024]{1,0:T(8,128)(2,1)} %tokens_h.1, f32[1,2048]{1,0:T(1,128)} %bitcast.19, f32[1,1024]{1,0:T(1,128)} %bitcast.20, bf16[8,128]{1,0:T(8,128)(2,1)} %bitcast.21, s32[2,16]{1,0:T(2,128)} %bitcast.22, bf16[2,16]{1,0:T(2,128)(2,1)} %bitcast.23, ...), custom_call_target="tpu_custom_call" | custom-call | tf_op jit(solution)/shard_map/layer/pallas_call | solution.py:638
  56.3 0.6 %copy.21 = bf16[16,1024]{1,0:T(8,128)(2,1)} copy(bf16[16,1024]{1,0:T(8,128)(2,1)S(1)} %get-tuple-element.2) | data formatting | bytes 65536
  56.9 1.3 %copy.22 = f32[16,2,128,128]{3,2,1,0:T(8,128)} copy(f32[16,2,128,128]{3,2,1,0:T(8,128)S(1)} %get-tuple-element.3) | data formatting | bytes 4194304

commit v5 on v4

--- a/solution.py
+++ b/solution.py
@@ -177,7 +177,7 @@
     barrier = pltpu.get_barrier_semaphore()
     peers = [partner]
     for by in (1, -1):
-        peers += [along_z(by), along_p(by), along_q(by)]
+        peers += [along_z(by), along_z(2 * by), along_p(by), along_q(by)]
     for peer in peers:
         pl.semaphore_signal(barrier, inc=1, device_id=peer, device_id_type=MESH)
 
@@ -197,16 +197,10 @@
     def hear(n):
         pl.semaphore_wait(known.at[n], 1)
 
-    tell(0, along_z(1))
-    tell(3, along_z(-1))
-    tell(6, along_p(1))
-    tell(7, along_q(1))
-
-    def relay(n):
-        for start, by in ((0, 1), (3, -1)):
-            hear(start + n)
-            tell(start + n + 1, along_z(by))
-
+    tell(0, along_z(2))
+    tell(1, along_z(-2))
+    tell(2, along_p(1))
+    tell(3, along_q(1))
 
     pair = [started(tokens, tok_p, partner), started(norm_ffn, nf_p, partner)]
 
@@ -240,7 +234,6 @@
     blank = jnp.zeros((112, 256), F32)
     query_t = jnp.concatenate([query, blank], axis=0).T
     key_t = jnp.concatenate([key, blank], axis=0).T
-    relay(0)
     loads[12].wait()
     decay = [jnp.where(first, 1.0 - 2.0 ** (-3.0 - 2.0 * h), 1.0 - 2.0 ** (-7.0 - 2.0 * h)) for h in range(2)]
     for h in range(2):
@@ -278,15 +271,14 @@
     extra = jnp.where(first, extra[0:32, :], extra[32:64, :]).astype(BF16)
     mine = jnp.where(first, chosen[0:32, :], chosen[32:64, :]).astype(BF16)
 
-    relay(1)
     mix_copy.wait_recv()
     after = (full + (mix_o[...].astype(F32) + mix_p[...].astype(F32))).astype(BF16).astype(F32)
     mean2 = jnp.sum(after * after, axis=1, keepdims=True) / 2048.0
     nf_lo, nf_hi = halves(norm_ffn[...], nf_p[...])
     normed2 = (after * lax.rsqrt(mean2 + epsilon) * jnp.concatenate([nf_lo, nf_hi], axis=1)).astype(BF16)
 
-    hear(2)
-    hear(5)
+    hear(0)
+    hear(1)
     rows = dot(mine, normed2)
     disp[:, 2048:2176] = extra
     disp[:, 0:2048] = rows.astype(BF16)
@@ -311,19 +303,19 @@
         for s in range(16):
             st[s, h] = decay[h] * st[s, h] + key_t[span, s : s + 1] * value[s : s + 1, span]
 
+    for j in (1, 2, 3):
+        moved[j].wait_recv()
+
+    @pl.when(jnp.logical_not(first))
+    def _():
+        moved[0].wait_recv()
+
     ring[1].wait_recv()
     forward(1, 2)
     ring[7].wait_recv()
     forward(7, 6)
     across(1)
     across(7)
-    for j in (1, 2, 3):
-        moved[j].wait_recv()
-
-    @pl.when(jnp.logical_not(first))
-    def _():
-        moved[0].wait_recv()
-
     def cell(ref, rq, rp):
         return ref.at[4 * AT[rq] + rp]
 
@@ -371,29 +363,33 @@
         arrived(2 - by, rp, n)
         spread(2 - by, rp, 2, rp, n, along_q(by))
 
-    hear(6)
-    hear(7)
+    hear(2)
+    hear(3)
     for n in range(2):
         spread(0, 0, 0, 1, n, along_p(1))
         spread(0, 0, 0, 3, n, along_p(-1))
         send_q(0, n)
+    for n in range(2):
         spread(0, 0, 0, 2, n, along_p(2))
-    for n in range(2):
+    def pass_first(n):
         arrived(0, 1, n)
         send_q(1, n)
         arrived(0, 3, n)
         send_q(3, n)
         pass_on(0, n)
-    for n in range(2):
-        arrived(0, 2, n)
-        send_q(2, n)
-        spread(0, 2, 2, 2, n, along_q(2))
+
+    pass_first(0)
     ring[2].wait_recv()
     forward(2, 3)
     ring[6].wait_recv()
     forward(6, 5)
     across(2)
     across(6)
+    pass_first(1)
+    for n in range(2):
+        arrived(0, 2, n)
+        send_q(2, n)
+        spread(0, 2, 2, 2, n, along_q(2))
     for n in (14, 15, 16):
         loads[n].wait()
     for copy in swap:
@@ -435,23 +431,23 @@
     for n in range(2):
         pass_on(1, n)
         pass_on(3, n)
-    for n in (3, 5):
-        ring[n].wait_recv()
-        across(n)
-    for copy in cross.values():
-        copy.wait_recv()
-    own_d = dense_rows(own, 12, 4)
     for n in range(2):
         for rp in range(4):
             for rq in (1, 3):
                 if rp == 2 or PASS[rp] != 2 - rq:
                     arrived(rq, rp, n)
+    near_e = expert_rows(operands(4, 8), 4, 8)
+    for n in (3, 5):
+        ring[n].wait_recv()
+        across(n)
     for n in range(2):
         for rp in range(4):
             arrived(2, rp, n)
-    rest = operands(0, 12)
-    rest_e = expert_rows(rest, 0, 12)
-    rest_d = dense_rows(rest, 0, 12)
+    far = operands(0, 4)
+    far_e = expert_rows(far, 0, 4)
+    for copy in cross.values():
+        copy.wait_recv()
+    far_d = dense_rows(far, 0, 4)
 
     def blocks(rows, start, count):
         return jnp.concatenate(
@@ -497,9 +493,10 @@
             if rp == 2 or PASS[rp] != 2 - rq:
                 send_back(rq, rp, n)
 
-    down(blocks(rest_e, 0, 4), blocks(rest_d, 0, 4), 0, 4, send_far)
-    down(blocks(rest_e, 4, 8), blocks(rest_d, 4, 8), 4, 8, send_near)
-    down(own_e, own_d, 12, 4, lambda n: None)
+    down(far_e, far_d, 0, 4, send_far)
+    rest_d = dense_rows(operands(4, 12), 4, 12)
+    down(near_e, blocks(rest_d, 0, 8), 4, 8, send_near)
+    down(own_e, blocks(rest_d, 8, 4), 12, 4, lambda n: None)
     for n in range(2):
         for rp in (1, 3, 0):
             rq = 2 - PASS[rp]
@@ -680,7 +677,7 @@
             pltpu.SemaphoreType.DMA((COPIES,)),
             pltpu.SemaphoreType.DMA((8,)),
             pltpu.SemaphoreType.DMA((8,)),
-            pltpu.SemaphoreType.REGULAR((8,)),
+            pltpu.SemaphoreType.REGULAR((4,)),
         ],
         compiler_params=pltpu.CompilerParams(collective_id=0, has_side_effects=True, vmem_limit_bytes=56 * 1024 * 1024),
         name="layer",

time: 58.3 us -> 57 us (0.978)
  Pallas kernels: 55.6 us -> 54.3 us
    pallas_call x1, Pallas kernels: 55.6 us -> 54.3 us  [body(): pl.pallas_call(kernel, out_shape=(pltpu.VMEM(tokens.shape, tokens.dtype),...]
where the time goes in v5:
time: 57 us; the launch traced here: 56.9 us
  Pallas kernels  54.3 us (95%)
  local copies, waits for them, and re-layouts  1.94 us (3%)
  between operations  0.65 us (1%)
    pallas_call x1, Pallas kernels, body(): pl.pallas_call(kernel, out_shape=(pltpu.VMEM(tokens.shape, tokens.dtype),...  54.3 us
    unnamed x2, local copies, waits for them, and re-layouts  1.94 us

profile of v5, /device:TPU:1, one launch (start us, length us, event | category | flops | bytes accessed | tf_op | source)
XLA Modules:
  0.0 56.9 jit_solution(16427260221982412107)
XLA Ops:
  0.6 54.3 %layer.1 = (bf16[16,1024]{1,0:T(8,128)(2,1)S(1)}, f32[16,2,128,128]{3,2,1,0:T(8,128)S(1)}) custom-call(bf16[16,1024]{1,0:T(8,128)(2,1)} %tokens_h.1, f32[1,2048]{1,0:T(1,128)} %bitcast.19, f32[1,1024]{1,0:T(1,128)} %bitcast.20, bf16[8,128]{1,0:T(8,128)(2,1)} %bitcast.21, s32[2,16]{1,0:T(2,128)} %bitcast.22, bf16[2,16]{1,0:T(2,128)(2,1)} %bitcast.23, ...), custom_call_target="tpu_custom_call" | custom-call | tf_op jit(solution)/shard_map/layer/pallas_call | solution.py:635
  55.0 0.6 %copy.21 = bf16[16,1024]{1,0:T(8,128)(2,1)} copy(bf16[16,1024]{1,0:T(8,128)(2,1)S(1)} %get-tuple-element.2) | data formatting | bytes 65536
  55.6 1.3 %copy.22 = f32[16,2,128,128]{3,2,1,0:T(8,128)} copy(f32[16,2,128,128]{3,2,1,0:T(8,128)S(1)} %get-tuple-element.3) | data formatting | bytes 4194304

commit v6 on v5

--- a/solution.py
+++ b/solution.py
@@ -607,6 +607,17 @@
     assert used[0] <= COPIES
 
 
+def leave(mixed, state, mixed_out, state_out, sem):
+    copies = [pltpu.make_async_copy(mixed, mixed_out, sem.at[8])]
+    for n in range(8):
+        part = pl.ds(2 * n, 2)
+        copies.append(pltpu.make_async_copy(state.at[part], state_out.at[part], sem.at[n]))
+    for copy in copies:
+        copy.start()
+    for copy in copies:
+        copy.wait()
+
+
 def body(
     tokens,
     state,
@@ -632,7 +643,7 @@
     def buf(*shape, dtype=BF16):
         return pltpu.VMEM(shape, dtype)
 
-    return pl.pallas_call(
+    results = pl.pallas_call(
         kernel,
         out_shape=(
             pltpu.VMEM(tokens.shape, tokens.dtype),
@@ -705,6 +716,18 @@
             )
         )
     )
+    return pl.pallas_call(
+        leave,
+        out_shape=(
+            jax.ShapeDtypeStruct(tokens.shape, tokens.dtype),
+            jax.ShapeDtypeStruct(state.shape, state.dtype),
+        ),
+        in_specs=[vmem, vmem],
+        out_specs=(hbm, hbm),
+        scratch_shapes=[pltpu.SemaphoreType.DMA((9,))],
+        name="leave",
+        compiler_params=pltpu.CompilerParams(vmem_limit_bytes=4 * 1024 * 1024),
+    )(*(pltpu.with_memory_space_constraint(result, pltpu.VMEM) for result in results))
 
 
 def solution(mesh):

time: 57 us -> 56.4 us (0.989)
  local copies, waits for them, and re-layouts: 1.94 us -> 0 us
  Pallas kernels: 54.3 us -> 55.7 us
    unnamed x2 -> x0, local copies, waits for them, and re-layouts: 1.94 us -> none
    pallas_call x0 -> x1, Pallas kernels: none -> 1.4 us  [body(): pl.pallas_call(leave, out_shape=(jax.ShapeDtypeStruct(tokens.shape, token...]
where the time goes in v6:
time: 56.4 us
  Pallas kernels  55.7 us (99%)
  between operations  0.65 us (1%)
    pallas_call x1, Pallas kernels, body(): pl.pallas_call(kernel, out_shape=(pltpu.VMEM(tokens.shape, tokens.dtype),...  54.3 us
    pallas_call x1, Pallas kernels, body(): pl.pallas_call(leave, out_shape=(jax.ShapeDtypeStruct(tokens.shape, token...  1.4 us

profile of v6, /device:TPU:1, one launch (start us, length us, event | category | flops | bytes accessed | tf_op | source)
XLA Modules:
  0.0 56.4 jit_solution(1536995380346879243)
XLA Ops:
  0.6 54.3 %layer.1 = (bf16[16,1024]{1,0:T(8,128)(2,1)S(1)}, f32[16,2,128,128]{3,2,1,0:T(8,128)S(1)}) custom-call(bf16[16,1024]{1,0:T(8,128)(2,1)} %tokens_h.1, f32[1,2048]{1,0:T(1,128)} %bitcast.19, f32[1,1024]{1,0:T(1,128)} %bitcast.20, bf16[8,128]{1,0:T(8,128)(2,1)} %bitcast.21, s32[2,16]{1,0:T(2,128)} %bitcast.22, bf16[2,16]{1,0:T(2,128)(2,1)} %bitcast.23, ...), custom_call_target="tpu_custom_call" | custom-call | tf_op jit(solution)/shard_map/layer/pallas_call | solution.py:646
  55.0 1.4 %leave.1 = (bf16[16,1024]{1,0:T(8,128)(2,1)}, f32[16,2,128,128]{3,2,1,0:T(8,128)}) custom-call(bf16[16,1024]{1,0:T(8,128)(2,1)S(1)} %get-tuple-element.4.mixed, f32[16,2,128,128]{3,2,1,0:T(8,128)S(1)} %get-tuple-element.5.state), custom_call_target="tpu_custom_call" | custom-call | tf_op jit(solution)/shard_map/leave/pallas_call | solution.py:719
